TPU v7x, 32 devices: a whole 2x2x4 slice. The times are simulated.
32 devices in a mesh: sp: 8 (over z, core), tp: 4 (over y, x).
Axes of the slice: x: 2, y: 2, z: 4, core: 2. Of those that a mesh axis runs over, the one named last changes fastest.
Arguments:
- cotangent: bfloat16 [1024, 2048], P('sp'), may hold values from -6 to 6
- normed: bfloat16 [1024, 2048], P('sp'), may hold values from -6 to 6
- inverse_root_mean_square: float32 [1024], P('sp'), may hold values from 0.5 to 2
- expert_norm_scale: float32 [2048], replicated, may hold values from 0.1 to 1.9
- routes: int32 [1024, 2], P('sp'), may hold values from 0 to 7, all different within a row; in each aligned block of 128 rows (0 to 127, 128 to 255, ...) at most 64 rows name the same one
- route_probability_weight: float32 [1024, 2], P('sp'), may hold values from 0.2 to 1
- gate_weight: bfloat16 [8, 2048, 2048], P('sp', None, 'tp'), may hold values from -0.125 to 0.125
- up_weight: bfloat16 [8, 2048, 2048], P('sp', None, 'tp'), may hold values from -0.125 to 0.125
- down_weight: bfloat16 [8, 2048, 2048], P('sp', 'tp'), may hold values from -0.125 to 0.125
- recurrence_input: bfloat16 [1024, 1024], P('sp', 'tp'), may hold values from -6 to 6
- recurrence_gate_logits: bfloat16 [1024, 1024], P('sp', 'tp'), may hold values from -6 to 6
- input_gate_logits: bfloat16 [1024, 1024], P('sp', 'tp'), may hold values from -6 to 6
- channel_decay_weight: float32 [1024], P('tp'), may hold values from 3 to 20
- extra_log_decay: float32 [1024, 1024], P('sp', 'tp'), may hold values from -1 to 0
- output_matrix: bfloat16 [2048, 1024], P(None, 'tp'), may hold values from -0.1875 to 0.1875
Outputs:
- grad_gate: bfloat16 [8, 2048, 2048], P('sp', None, 'tp')
- grad_up: bfloat16 [8, 2048, 2048], P('sp', None, 'tp')
- grad_down: bfloat16 [8, 2048, 2048], P('sp', 'tp')
- grad_out_weight: float32 [2048, 1024], P('sp', 'tp')
- grad_rec_input: float32 [1024, 1024], P('sp', 'tp')
- grad_decay_gate: float32 [1024, 1024], P('sp', 'tp')
- grad_input_gate: float32 [1024, 1024], P('sp', 'tp')
Inputs may be any that keep to these rules, and one draw needn't show every extreme that they name: `routes`: each row names 2 different experts; among the rows of one device no expert is named more than 64 times.
All inputs are finite; a program needn't handle non-finite values.
Results may differ from a plain program's by a relative error of at most 0.025.
Values may be sent and summed in bfloat16 or wider, within the bound.
A program may use at most 64 MiB of HBM per device.

v0:
```python
import functools

import jax
import jax.numpy as jnp
from jax import lax
from jax.experimental import pallas as pl
from jax.experimental.pallas import tpu as pltpu
from jax.sharding import PartitionSpec as P

MESH = pl.DeviceIdType.MESH
VMEM_LIMIT = 56 * 1024 * 1024


def sides(m):
    high = max(d for d in range(1, m + 1) if m % d == 0 and d * d <= m)
    return high, m // high


def greet(n, m, me, j):
    barrier = pltpu.get_barrier_semaphore()
    for k in range(1, n):
        pl.semaphore_signal(
            barrier, inc=1, device_id={"sp": lax.rem(me + k, n)}, device_id_type=MESH
        )
    for p in range(1, m):
        pl.semaphore_signal(
            barrier, inc=1, device_id={"tp": lax.rem(j + p, m)}, device_id_type=MESH
        )
    pl.semaphore_wait(barrier, n - 1 + m - 1)


def send(src, dst, send_sem, recv_sem, where):
    return pltpu.make_async_remote_copy(
        src_ref=src,
        dst_ref=dst,
        send_sem=send_sem,
        recv_sem=recv_sem,
        device_id=where,
        device_id_type=MESH,
    )


def scan_rows(a, b, reverse):
    rows = a.shape[0]
    place = lax.broadcasted_iota(jnp.int32, a.shape, 0)
    step = 1
    while step < rows:
        if reverse:
            known = place < rows - step
            shift = rows - step
        else:
            known = place >= step
            shift = step
        a_far = jnp.where(known, pltpu.roll(a, shift, 0), 1.0)
        b_far = jnp.where(known, pltpu.roll(b, shift, 0), 0.0)
        b = a * b_far + b
        a = a * a_far
        step *= 2
    return a, b


def dispatch_kernel(
    n, m, xs, ys, keep, driven, xo, yo, hidden, prev, carry,
    cum, loc, s1s, s1r, f1s, f1r, f2s, f2r, cs, cr, lsem,
):
    me, j = lax.axis_index("sp"), lax.axis_index("tp")
    cap, q = xs.shape[0] // n, xs.shape[1]
    tok = keep.shape[0]
    rows = lambda s: pl.ds(pl.multiple_of(s * cap, cap), cap)
    cols = lambda t: pl.ds(pl.multiple_of(t * q, q), q)
    pairs = ((0, xs, xo), (1, ys, yo))
    high, low = sides(m)
    upper, lower = lax.div(j, low), lax.rem(j, low)

    def size(i):
        return low if i == 0 else high

    def near(i, along, across):
        up, down = (across, along) if i == 0 else (along, across)
        return lax.rem(upper + up, high) * low + lax.rem(lower + down, low)

    a, b = scan_rows(keep[...], driven[...], False)
    cum[...] = a
    loc[...] = b
    width = a.shape[1]
    carry[me] = jnp.concatenate(
        [a[tok - 1 : tok], b[tok - 1 : tok], jnp.zeros((6, width), jnp.float32)], axis=0
    )
    greet(n, m, me, j)

    def first(k):
        to = lax.rem(me + k, n)
        return [
            send(s.at[rows(to)], o.at[rows(me), cols(j)], s1s.at[i], s1r.at[i, k], {"sp": to})
            for i, s, o in pairs
        ]

    def carried(k):
        to = lax.rem(me + k, n)
        return send(carry.at[me], carry.at[me], cs.at[k], cr.at[k], {"sp": to})

    own = [
        pltpu.make_async_copy(s.at[rows(me)], o.at[rows(me), cols(j)], lsem.at[i])
        for i, s, o in pairs
    ]
    for c in own:
        c.start()

    def start_carry(k, _):
        carried(k).start()
        return 0

    lax.fori_loop(1, n, start_carry, 0)

    def start_first(k, _):
        for c in first(k):
            c.start()
        return 0

    lax.fori_loop(1, n, start_first, 0)

    def onward(k, i, o):
        source = lax.rem(me - k + n, n)
        block = o.at[rows(source), cols(j)]
        for p in range(1, size(i)):
            send(block, block, f1s.at[i, p], f1r.at[i, p, k], {"tp": near(i, p, 0)}).start()
        for p in range(1, size(1 - i)):
            send(block, block, f2s.at[i, p, 0], f2r.at[i, p, 0], {"tp": near(i, 0, p)}).start()

    def relayed(k, i, o):
        source = lax.rem(me - k + n, n)
        for c in range(1, size(i)):
            far = near(i, size(i) - c, 0)
            block = o.at[rows(source), cols(far)]
            send(block, block, f1s.at[i, c], f1r.at[i, c, k], {"tp": far}).wait_recv()
            for p in range(1, size(1 - i)):
                send(block, block, f2s.at[i, p, c], f2r.at[i, p, c], {"tp": near(i, 0, p)}).start()

    for c in own:
        c.wait()
    for i, _, o in pairs:
        onward(0, i, o)

    def relay(k, _):
        source = lax.rem(me - k + n, n)
        for i, s, o in pairs:
            block = o.at[rows(source), cols(j)]
            send(block, block, s1s.at[i], s1r.at[i, k], {"sp": source}).wait_recv()
            onward(k, i, o)
        for i, s, o in pairs:
            relayed(k - 1, i, o)
        return 0

    lax.fori_loop(1, n, relay, 0)
    for i, _, o in pairs:
        relayed(n - 1, i, o)

    def take_carry(k, _):
        source = lax.rem(me - k + n, n)
        send(carry.at[source], carry.at[source], cs.at[k], cr.at[k], {"sp": source}).wait_recv()
        carried(k).wait_send()
        return 0

    lax.fori_loop(1, n, take_carry, 0)
    state = jnp.zeros((1, width), jnp.float32)
    for s in range(n):
        state = jnp.where(s < me, carry[s, 0:1] * state + carry[s, 1:2], state)
    whole = loc[...] + cum[...] * state
    hidden[...] = whole.astype(hidden.dtype)
    place = lax.broadcasted_iota(jnp.int32, whole.shape, 0)
    prev[...] = jnp.where(place >= 1, pltpu.roll(whole, 1, 0), state)
    for i, s, o in pairs:
        part = s.at[pl.ds(0, (n - 1) * cap)]
        send(part, part, s1s.at[i], s1r.at[i, 0], {"sp": lax.rem(me + 1, n)}).wait_send()
        mine = o.at[:, cols(j)]
        for p in range(1, size(i)):
            send(mine, mine, f1s.at[i, p], f1r.at[i, p, 0], {"tp": near(i, p, 0)}).wait_send()
        for p in range(1, size(1 - i)):
            for c in range(size(i)):
                sent = o.at[:, cols(near(i, size(i) - c, 0))]
                came = o.at[:, cols(near(i, size(i) - c, size(1 - i) - p))]
                to = {"tp": near(i, 0, p)}
                send(sent, sent, f2s.at[i, p, c], f2r.at[i, p, c], to).wait_send()
                send(came, came, f2s.at[i, p, c], f2r.at[i, p, c], to).wait_recv()


def return_kernel(
    n, m, pr, pick, hid, cot, nrm, gain, irms, omat, keep, carry, total_out, gow,
    out, hid_all, stage, red, back, mix_t, got, cum, loc, enters,
    rs, rr, bs, br, gs, gr, hs, hr, ms, mr, cs, cr, lsem,
):
    me, j = lax.axis_index("sp"), lax.axis_index("tp")
    tok = hid.shape[0]
    cap, q = pr.shape[0] // n, pr.shape[1] // m
    rows = lambda s: pl.ds(pl.multiple_of(s * cap, cap), cap)
    cols = lambda t: pl.ds(pl.multiple_of(t * q, q), q)
    greet(n, m, me, j)
    own = pltpu.make_async_copy(hid, hid_all.at[me], lsem)
    own.start()

    def spread(k, _):
        to = lax.rem(me + k, n)
        for p in range(1, m):
            far = lax.rem(j + p, m)
            send(
                pr.at[rows(to), cols(far)],
                stage.at[p - 1, rows(to)],
                rs.at[k],
                rr.at[k],
                {"tp": far},
            ).start()
        return 0

    lax.fori_loop(1, n + 1, spread, 0)

    def share(k, _):
        to = lax.rem(me + k, n)
        send(hid, hid_all.at[me], hs.at[k], hr.at[k], {"sp": to}).start()
        return 0

    lax.fori_loop(1, n, share, 0)

    def ship(k):
        to = lax.rem(me + k, n)
        return send(red.at[rows(to)], back.at[rows(me)], bs.at[k], br.at[k], {"sp": to})

    def reduce(k, _):
        to = lax.rem(me + k, n)
        block = stage.at[:, rows(to)]
        got = send(block, block, rs.at[k], rr.at[k], {"tp": lax.rem(j + 1, m)})
        got.wait_recv()
        got.wait_send()
        total = pr[rows(to), cols(j)].astype(jnp.float32)
        for p in range(1, m):
            total = total + stage[p - 1, rows(to)].astype(jnp.float32)
        red[rows(to)] = total.astype(red.dtype)

        @pl.when(k > 1)
        def _():
            ship(k - 1).start()

        return 0

    lax.fori_loop(1, n + 1, reduce, 0)
    back[rows(me)] = red[rows(me)]

    def collect(k, _):
        source = lax.rem(me - k + n, n)
        block = back.at[rows(source)]
        send(block, block, bs.at[k], br.at[k], {"sp": source}).wait_recv()
        return 0

    lax.fori_loop(1, n, collect, 0)
    total = jnp.dot(pick[...], back[...], preferred_element_type=jnp.float32)
    out[:, cols(j)] = total.astype(out.dtype)

    def finish(k, _):
        source = lax.rem(me - k + n, n)
        ship(k).wait_send()
        got = send(hid, hid_all.at[source], hs.at[k], hr.at[k], {"sp": source})
        got.wait_recv()
        got.wait_send()
        return 0

    lax.fori_loop(1, n, finish, 0)
    own.wait()
    mine = out.at[:, cols(j)]
    for p in range(1, m):
        send(mine, mine, gs.at[p], gr.at[p], {"tp": lax.rem(j + p, m)}).start()
    for p in range(1, m):
        far = lax.rem(j - p + m, m)
        theirs = out.at[:, cols(far)]
        send(mine, mine, gs.at[p], gr.at[p], {"tp": far}).wait_send()
        send(theirs, theirs, gs.at[p], gr.at[p], {"tp": far}).wait_recv()

    slab = mix_t.shape[0] // n
    width = keep.shape[1]
    slabs = lambda s: pl.ds(pl.multiple_of(s * slab, slab), slab)
    scale = gain[...]
    nhat = nrm[...].astype(jnp.float32) / scale
    gained = scale * out[...].astype(jnp.float32)
    stat = jnp.mean(gained * nhat, axis=1, keepdims=True)
    mixed = cot[...].astype(jnp.float32) + irms[...] * (gained - nhat * stat)
    mix_t[...] = mixed.T.astype(mix_t.dtype)
    loc[...] = jnp.dot(
        mixed.astype(omat.dtype), omat[...], preferred_element_type=jnp.float32
    )

    def blocks(k):
        to = lax.rem(me + k, n)
        return send(mix_t.at[slabs(to)], got.at[me], ms.at[k], mr.at[k], {"sp": to})

    def carried(k):
        to = lax.rem(me + k, n)
        return send(enters.at[me], enters.at[me], cs.at[k], cr.at[k], {"sp": to})

    def start_blocks(k, _):
        blocks(k).start()
        return 0

    lax.fori_loop(1, n, start_blocks, 0)
    place = lax.broadcasted_iota(jnp.int32, (tok, width), 0)
    here = keep[...]
    after = jnp.where(place < tok - 1, pltpu.roll(here, tok - 1, 0), 1.0)
    a, b = scan_rows(after, loc[...], True)
    enters[me] = jnp.broadcast_to(here[0:1] * b[0:1], (8, width))
    cum[...] = a
    loc[...] = b
    gow[...] = jnp.dot(mix_t[slabs(me)], hid_all[me], preferred_element_type=jnp.float32)

    def start(k, _):
        carried(k).start()
        return 0

    lax.fori_loop(1, n, start, 0)

    def add(k, _):
        source = lax.rem(me - k + n, n)
        send(got.at[source], got.at[source], ms.at[k], mr.at[k], {"sp": source}).wait_recv()
        blocks(k).wait_send()
        gow[...] += jnp.dot(got[source], hid_all[source], preferred_element_type=jnp.float32)
        return 0

    lax.fori_loop(1, n, add, 0)

    def take(k, _):
        source = lax.rem(me - k + n, n)
        send(enters.at[source], enters.at[source], cs.at[k], cr.at[k], {"sp": source}).wait_recv()
        carried(k).wait_send()
        return 0

    lax.fori_loop(1, n, take, 0)
    enter = jnp.zeros((1, width), jnp.float32)
    for s in range(n - 1, -1, -1):
        enter = jnp.where(s > me, carry[s, 0:1] * enter + enters[s, 0:1], enter)
    total_out[...] = loc[...] + cum[...] * enter


def call(kernel, n, m, outs, scratch, ident, *args, loose=0):
    return pl.pallas_call(
        functools.partial(kernel, n, m),
        out_shape=tuple(jax.ShapeDtypeStruct(s, d) for s, d in outs),
        in_specs=[pl.BlockSpec(memory_space=pltpu.VMEM)] * len(args),
        out_specs=tuple(
            pl.BlockSpec(memory_space=pl.ANY if at < loose else pltpu.VMEM)
            for at in range(len(outs))
        ),
        scratch_shapes=scratch,
        compiler_params=pltpu.CompilerParams(
            collective_id=ident, has_side_effects=True, vmem_limit_bytes=VMEM_LIMIT
        ),
    )(*args)


def shards(
    cotangent,
    normed,
    inverse_root_mean_square,
    expert_norm_scale,
    routes,
    route_probability_weight,
    gate_weight,
    up_weight,
    down_weight,
    recurrence_input,
    recurrence_gate_logits,
    input_gate_logits,
    channel_decay_weight,
    extra_log_decay,
    output_matrix,
):
    tok_rows, features = normed.shape
    n, m = lax.axis_size("sp"), lax.axis_size("tp")
    picks = routes.shape[1]
    capacity = 2 * picks * tok_rows // n
    slots = n * capacity
    q = features // m
    wide = max(sides(m))
    channels = recurrence_input.shape[1]
    f32, bf16 = jnp.float32, jnp.bfloat16
    dma = pltpu.SemaphoreType.DMA
    rowdims = (((0,), (0,)), ((), ()))
    coldims = (((1,), (1,)), ((), ()))

    chosen = routes.reshape(-1)
    member = chosen[:, None] == jnp.arange(n, dtype=jnp.int32)[None, :]
    order = jnp.arange(chosen.shape[0])
    below = (order[:, None] > order[None, :]).astype(bf16)
    before = jnp.dot(below, member.astype(bf16), preferred_element_type=f32)
    ranking = jnp.sum(jnp.where(member, before, 0.0), axis=1).astype(jnp.int32)
    landing = (chosen * capacity + ranking).reshape(tok_rows, picks)
    slot = jnp.arange(slots, dtype=jnp.int32)
    hits = [slot[:, None] == landing[:, k][None, :] for k in range(picks)]
    place = functools.reduce(jnp.logical_or, hits).astype(bf16)
    pick = functools.reduce(
        jnp.logical_or, [landing[:, k][:, None] == slot[None, :] for k in range(picks)]
    ).astype(bf16)
    share = sum(
        jnp.sum(jnp.where(h, route_probability_weight[:, k][None, :], 0.0), axis=1)
        for k, h in enumerate(hits)
    )
    offset = lax.axis_index("tp") * q
    normed_part = lax.dynamic_slice_in_dim(normed, offset, q, 1)
    cot_part = lax.dynamic_slice_in_dim(cotangent, offset, q, 1)
    token_send = jnp.dot(place, normed_part, preferred_element_type=f32).astype(bf16)
    grad_send = (
        share[:, None] * jnp.dot(place, cot_part, preferred_element_type=f32)
    ).astype(bf16)

    retention_factor = jax.nn.sigmoid(recurrence_gate_logits.astype(f32))
    admit = jax.nn.sigmoid(input_gate_logits.astype(f32))
    signal = recurrence_input.astype(f32)
    decay_speed = jax.nn.softplus(-channel_decay_weight)
    log_retention = -8.0 * retention_factor * decay_speed[None, :] + extra_log_decay
    keep = jnp.exp(log_retention)
    scale_in = jnp.sqrt(-jnp.expm1(2.0 * log_retention))
    driven = scale_in * admit * signal

    token_recv, grad_recv, hidden, state_prev, carry = call(
        dispatch_kernel, n, m,
        [
            ((slots, features), bf16),
            ((slots, features), bf16),
            ((tok_rows, channels), bf16),
            ((tok_rows, channels), f32),
            ((n, 8, channels), f32),
        ],
        [
            pltpu.VMEM((tok_rows, channels), f32),
            pltpu.VMEM((tok_rows, channels), f32),
            dma((2,)),
            dma((2, n)),
            dma((2, wide)),
            dma((2, wide, n)),
            dma((2, wide, wide)),
            dma((2, wide, wide)),
            dma((n,)),
            dma((n,)),
            dma((2,)),
        ],
        0, token_send, grad_send, keep, driven, loose=2,
    )

    gate_w = gate_weight[0]
    up_w = up_weight[0]
    down_w = down_weight[0]
    gate_pre = jnp.dot(token_recv, gate_w, preferred_element_type=f32)
    up_pre = jnp.dot(token_recv, up_w, preferred_element_type=f32)
    sigma = jax.nn.sigmoid(gate_pre)
    swish = gate_pre * sigma
    active = (swish * up_pre).astype(bf16)
    d_active = lax.dot_general(grad_recv, down_w, coldims, preferred_element_type=f32)
    d_gate = (d_active * up_pre * sigma * (1.0 + gate_pre * (1.0 - sigma))).astype(bf16)
    d_up = (d_active * swish).astype(bf16)
    grad_down = lax.dot_general(active, grad_recv, rowdims, preferred_element_type=f32).astype(bf16)
    grad_gate = lax.dot_general(token_recv, d_gate, rowdims, preferred_element_type=f32).astype(bf16)
    grad_up = lax.dot_general(token_recv, d_up, rowdims, preferred_element_type=f32).astype(bf16)
    partial_rows = lax.dot_general(d_gate, gate_w, coldims, preferred_element_type=f32)
    partial_rows = partial_rows + lax.dot_general(d_up, up_w, coldims, preferred_element_type=f32)

    total, grad_out_weight = call(
        return_kernel, n, m,
        [((tok_rows, channels), f32), ((features // n, channels), f32)],
        [
            pltpu.VMEM((tok_rows, features), bf16),
            pltpu.VMEM((n, tok_rows, channels), bf16),
            pltpu.VMEM((m - 1, slots, q), bf16),
            pltpu.VMEM((slots, q), bf16),
            pltpu.VMEM((slots, q), bf16),
            pltpu.VMEM((features, tok_rows), bf16),
            pltpu.VMEM((n, features // n, tok_rows), bf16),
            pltpu.VMEM((tok_rows, channels), f32),
            pltpu.VMEM((tok_rows, channels), f32),
            pltpu.VMEM((n, 8, channels), f32),
            dma((n + 1,)),
            dma((n + 1,)),
            dma((n,)),
            dma((n,)),
            dma((m,)),
            dma((m,)),
            dma((n,)),
            dma((n,)),
            dma((n,)),
            dma((n,)),
            dma((n,)),
            dma((n,)),
            dma,
        ],
        1,
        partial_rows.astype(bf16),
        pick,
        hidden,
        cotangent,
        normed,
        expert_norm_scale[None, :],
        inverse_root_mean_square[:, None],
        output_matrix,
        keep,
        carry,
    )
    grad_rec_input = total * scale_in * admit
    grad_input_gate = total * scale_in * signal * admit * (1.0 - admit)
    d_log = total * state_prev * keep - total * admit * signal * keep * keep / scale_in
    grad_decay_gate = (
        d_log * (-8.0 * decay_speed[None, :]) * retention_factor * (1.0 - retention_factor)
    )
    return (
        grad_gate[None],
        grad_up[None],
        grad_down[None],
        grad_out_weight,
        grad_rec_input,
        grad_decay_gate,
        grad_input_gate,
    )


def solution(mesh):
    return jax.shard_map(
        shards,
        mesh=mesh,
        in_specs=(
            P("sp", None),
            P("sp", None),
            P("sp"),
            P(),
            P("sp", None),
            P("sp", None),
            P("sp", None, "tp"),
            P("sp", None, "tp"),
            P("sp", "tp", None),
            P("sp", "tp"),
            P("sp", "tp"),
            P("sp", "tp"),
            P("tp"),
            P("sp", "tp"),
            P(None, "tp"),
        ),
        out_specs=(
            P("sp", None, "tp"),
            P("sp", None, "tp"),
            P("sp", "tp", None),
            P("sp", "tp"),
            P("sp", "tp"),
            P("sp", "tp"),
            P("sp", "tp"),
        ),
        check_vma=False,
    )
```

profile of v0, /device:TPU:0, one launch (start us, length us, event | category | flops | bytes accessed | tf_op | source)
XLA Modules:
  0.0 145.0 jit_solution(3715386336018353279)
XLA Ops:
  0.7 0.9 copy.35
  2.1 0.7 multiply_add_fusion.1
  2.9 2.0 %convolution_convert_fusion.3.xs = bf16[512,512]{1,0:T(8,128)(2,1)} fusion(bf16[128,2048]{1,0:T(8,128)(2,1)} %nrm.1, s32[]{:T(128)S(6)} %select_n.20, s32[128]{0:T(128)S(1)} %get-tuple-element.31, s32[128]{0:T(128)S(1)} %get-tuple-element.30), kind=kOutput, calls=%fused_computation.18 | convolution fusion | flops 67567616 | bytes 656388 | tf_op jit(solution)/shard_map/dot_general | solution.py:405
  4.9 0.8 slice_bitcast_fusion
  5.6 0.2 select_reduce_fusion
  5.8 2.0 %fusion.12.ys = bf16[512,512]{1,0:T(8,128)(2,1)} fusion(f32[512]{0:T(512)S(1)} %add.39, bf16[128,2048]{1,0:T(8,128)(2,1)} %cot.1, s32[]{:T(128)S(6)} %select_n.20, s32[128]{0:T(128)S(1)} %get-tuple-element.31, s32[128]{0:T(128)S(1)} %get-tuple-element.30), kind=kOutput, calls=%fused_computation.17 | convolution fusion | flops 67829760 | bytes 658436 | tf_op jit(solution)/shard_map/dot_general | solution.py:407
  7.8 0.7 fusion.37
  8.5 1.8 %convert_multiply_fusion.2 = (f32[128,256]{1,0:T(8,128)}, f32[128,256]{1,0:T(8,128)}) fusion(bf16[128,256]{1,0:T(8,128)(2,1)} %param.24, bf16[128,256]{1,0:T(8,128)(2,1)} %param.26, f32[128,256]{1,0:T(8,128)} %param.28, f32[256]{0:T(256)S(1)} %fusion.37, bf16[128,256]{1,0:T(8,128)(2,1)} %param.25), kind=kLoop, calls=%fused_computation.39 | loop fusion | flops 491520 | bytes 590848 | tf_op jit(solution)/shard_map/mul | solution.py:417
  10.4 49.9 %shard_map.198 = (bf16[512,2048]{1,0:T(8,128)(2,1)}, bf16[512,2048]{1,0:T(8,128)(2,1)}, bf16[128,256]{1,0:T(8,128)(2,1)}, f32[128,256]{1,0:T(8,128)}, f32[8,8,256]{2,1,0:T(8,128)}) custom-call(bf16[512,512]{1,0:T(8,128)(2,1)} %convolution_convert_fusion.3.xs, bf16[512,512]{1,0:T(8,128)(2,1)} %fusion.12.ys, f32[128,256]{1,0:T(8,128)} %get-tuple-element.27.keep, ...), custom_call_target="tpu_custom_call" | custom-call | tf_op jit(solution)/shard_map/pallas_call | solution.py:340
  60.3 3.0 %fusion.5 = f32[512,512]{1,0:T(8,128)S(1)} fusion(bf16[512,2048]{1,0:T(8,128)(2,1)} %get-tuple-element.14, bf16[1,2048,512]{2,1,0:T(8,128)(2,1)S(1)} %copy-done), kind=kOutput, calls=%fused_computation.9 | convolution fusion | flops 1073741824 | bytes 5242880 | tf_op jit(solution)/shard_map/dot_general | solution.py:447
  63.3 1.3 fusion.8
  64.6 0.3 copy-done.8
  64.9 0.6 copy-done.9
  65.5 1.6 %multiply_convert_fusion.1 = (bf16[512,512]{1,0:T(8,128)(2,1)S(1)}, bf16[512,512]{1,0:T(8,128)(2,1)S(1)}) fusion(f32[512,512]{1,0:T(8,128)S(1)} %fusion.5, f32[512,512]{1,0:T(8,128)S(1)} %fusion.8, bf16[512,2048]{1,0:T(8,128)(2,1)S(1)} %copy-done.9, bf16[1,512,2048]{2,1,0:T(8,128)(2,1)S(1)} %copy-done.8), kind=kOutput, calls=%fused_computation.22 | convolution fusion | flops 1077149696 | bytes 7340032 | tf_op jit(solution)/shard_map/dot_general | solution.py:452
  67.1 2.6 %fusion = bf16[1,2048,512]{2,1,0:T(8,128)(2,1)} fusion(bf16[512,2048]{1,0:T(8,128)(2,1)S(1)} %copy-done.10, bf16[512,512]{1,0:T(8,128)(2,1)S(1)} %get-tuple-element.22), kind=kOutput, calls=%fused_computation.4 | convolution fusion | flops 1074790400 | bytes 4718592 | tf_op jit(solution)/shard_map/dot_general | solution.py:456
  69.8 2.6 %fusion.1 = bf16[1,2048,512]{2,1,0:T(8,128)(2,1)} fusion(bf16[512,2048]{1,0:T(8,128)(2,1)S(1)} %copy-done.10, bf16[512,512]{1,0:T(8,128)(2,1)S(1)} %get-tuple-element.21), kind=kOutput, calls=%fused_computation.5 | convolution fusion | flops 1074790400 | bytes 4718592 | tf_op jit(solution)/shard_map/dot_general | solution.py:457
  72.4 2.7 %fusion.2 = bf16[1,512,2048]{2,1,0:T(8,128)(2,1)} fusion(bf16[512,2048]{1,0:T(8,128)(2,1)S(1)} %copy-done.9, f32[512,512]{1,0:T(8,128)S(1)} %fusion.8, f32[512,512]{1,0:T(8,128)S(1)} %fusion.5), kind=kOutput, calls=%fused_computation.6 | convolution fusion | flops 1076363264 | bytes 6291456 | tf_op jit(solution)/shard_map/dot_general | solution.py:455
  75.1 1.3 fusion.3
  76.5 2.6 %add_convert_fusion.pr = bf16[512,2048]{1,0:T(8,128)(2,1)} fusion(f32[512,2048]{1,0:T(8,128)S(1)} %fusion.3, bf16[512,512]{1,0:T(8,128)(2,1)S(1)} %get-tuple-element.21, bf16[1,2048,512]{2,1,0:T(8,128)(2,1)S(1)} %copy-done.1), kind=kOutput, calls=%fused_computation | convolution fusion | flops 1075838976 | bytes 8912896 | tf_op jit(solution)/shard_map/dot_general | solution.py:459
  79.1 0.8 fusion.17.pick
  79.8 0.7 copy.37.irms
  80.6 60.8 %shard_map.199 = (f32[128,256]{1,0:T(8,128)}, f32[256,256]{1,0:T(8,128)}) custom-call(bf16[512,2048]{1,0:T(8,128)(2,1)} %add_convert_fusion.pr, bf16[128,512]{1,0:T(8,128)(2,1)} %fusion.17.pick, bf16[128,256]{1,0:T(8,128)(2,1)} %get-tuple-element.16.hid, bf16[128,2048]{1,0:T(8,128)(2,1)} %cot.1, bf16[128,2048]{1,0:T(8,128)(2,1)} %nrm.1, f32[1,2048]{1,0:T(1,128)} %bitcast.41, ...), custom_call_target="tpu_custom_call" | custom-call | tf_op jit(solution)/shard_map/pallas_call | solution.py:340
  141.5 1.9 %fusion.22 = (f32[128,256]{1,0:T(8,128)}, f32[128,256]{1,0:T(8,128)}, f32[128,256]{1,0:T(8,128)}) fusion(bf16[128,256]{1,0:T(8,128)(2,1)S(1)} %copy-done.3, f32[128,256]{1,0:T(8,128)} %get-tuple-element.19, bf16[128,256]{1,0:T(8,128)(2,1)S(1)} %copy-done.4, f32[128,256]{1,0:T(8,128)S(1)} %copy-done.2, f32[256]{0:T(256)S(1)} %fusion.37, ...), kind=kLoop, calls=%fused_computation.41 | loop fusion | flops 1015808 | bytes 984064 | tf_op jit(solution)/shard_map/mul | solution.py:502
  143.4 1.7 %copy.39 = f32[256,256]{1,0:T(8,128)} copy(f32[256,256]{1,0:T(8,128)} %get-tuple-element.44) | data formatting | bytes 524288
  (27 shorter events, 0.6 us)
Async XLA Ops:
  0.6 59.6 %copy-start = (bf16[1,2048,512]{2,1,0:T(8,128)(2,1)S(1)}, bf16[1,2048,512]{2,1,0:T(8,128)(2,1)}, u32[]{:S(2)}) copy-start(bf16[1,2048,512]{2,1,0:T(8,128)(2,1)} %param.21) | copy-start | bytes 6291460
  60.3 3.0 %copy-start.1 = (bf16[1,2048,512]{2,1,0:T(8,128)(2,1)S(1)}, bf16[1,2048,512]{2,1,0:T(8,128)(2,1)}, u32[]{:S(2)}) copy-start(bf16[1,2048,512]{2,1,0:T(8,128)(2,1)} %param.22) | copy-start | bytes 6291460
  60.3 3.0 %copy-start.10 = (bf16[512,2048]{1,0:T(8,128)(2,1)S(1)}, bf16[512,2048]{1,0:T(8,128)(2,1)}, u32[]{:S(2)}) copy-start(bf16[512,2048]{1,0:T(8,128)(2,1)} %get-tuple-element.14) | copy-start | bytes 6291460
  63.3 1.6 %copy-start.8 = (bf16[1,512,2048]{2,1,0:T(8,128)(2,1)S(1)}, bf16[1,512,2048]{2,1,0:T(8,128)(2,1)}, u32[]{:S(2)}) copy-start(bf16[1,512,2048]{2,1,0:T(8,128)(2,1)} %param.23) | copy-start | bytes 6291460
  63.3 2.2 %copy-start.9 = (bf16[512,2048]{1,0:T(8,128)(2,1)S(1)}, bf16[512,2048]{1,0:T(8,128)(2,1)}, u32[]{:S(2)}) copy-start(bf16[512,2048]{1,0:T(8,128)(2,1)} %get-tuple-element.15) | copy-start | bytes 6291460
  76.5 3.4 %copy-start.7 = (f32[128]{0:T(128)S(1)}, f32[128]{0:T(128)}, u32[]{:S(2)}) copy-start(f32[128]{0:T(128)} %param.17) | copy-start | bytes 1540
  80.6 60.8 %copy-start.2 = (f32[128,256]{1,0:T(8,128)S(1)}, f32[128,256]{1,0:T(8,128)}, u32[]{:S(2)}) copy-start(f32[128,256]{1,0:T(8,128)} %param.28) | copy-start | bytes 393220
  80.6 60.8 %copy-start.3 = (bf16[128,256]{1,0:T(8,128)(2,1)S(1)}, bf16[128,256]{1,0:T(8,128)(2,1)}, u32[]{:S(2)}) copy-start(bf16[128,256]{1,0:T(8,128)(2,1)} %param.24) | copy-start | bytes 196612
  80.6 60.9 %copy-start.4 = (bf16[128,256]{1,0:T(8,128)(2,1)S(1)}, bf16[128,256]{1,0:T(8,128)(2,1)}, u32[]{:S(2)}) copy-start(bf16[128,256]{1,0:T(8,128)(2,1)} %param.26) | copy-start | bytes 196612
  80.6 60.9 %copy-start.5 = (bf16[128,256]{1,0:T(8,128)(2,1)S(1)}, bf16[128,256]{1,0:T(8,128)(2,1)}, u32[]{:S(2)}) copy-start(bf16[128,256]{1,0:T(8,128)(2,1)} %param.25) | copy-start | bytes 196612
  80.6 60.9 %copy-start.6 = (f32[128,256]{1,0:T(8,128)S(1)}, f32[128,256]{1,0:T(8,128)}, u32[]{:S(2)}) copy-start(f32[128,256]{1,0:T(8,128)} %get-tuple-element.20) | copy-start | bytes 393220
where the time goes:
time: 145 us
  Pallas kernels  111 us (77%)
  matrix products  22 us (15%)
  other arithmetic  6.11 us (4%)
  local copies, waits for them, and re-layouts  5.43 us (4%)
    pallas_call x2, Pallas kernels, call(): pl.pallas_call(functools.partial(kernel, n, m), out_shape=tuple((jax.Shap...  111 us
    unnamed x24, local copies, waits for them, and re-layouts  3.59 us
    dot_general x1, matrix products, shards(): gate_pre = jnp.dot(token_recv, gate_w, preferred_element_type=f32)  2.99 us

commit v1 on v0

v1 whole, which is shorter than its diff:
```python
import functools

import jax
import jax.numpy as jnp
from jax import lax
from jax.experimental import pallas as pl
from jax.experimental.pallas import tpu as pltpu
from jax.sharding import PartitionSpec as P

MESH = pl.DeviceIdType.MESH
VMEM_LIMIT = 63 * 1024 * 1024
F32, BF16 = jnp.float32, jnp.bfloat16
ROWDIMS = (((0,), (0,)), ((), ()))
COLDIMS = (((1,), (1,)), ((), ()))


def sides(m):
    high = max(d for d in range(1, m + 1) if m % d == 0 and d * d <= m)
    return high, m // high


def greet(n, m, me, j):
    barrier = pltpu.get_barrier_semaphore()
    for k in range(1, n):
        pl.semaphore_signal(
            barrier, inc=1, device_id={"sp": lax.rem(me + k, n)}, device_id_type=MESH
        )
    for p in range(1, m):
        pl.semaphore_signal(
            barrier, inc=1, device_id={"tp": lax.rem(j + p, m)}, device_id_type=MESH
        )
    pl.semaphore_wait(barrier, n - 1 + m - 1)


def send(src, dst, send_sem, recv_sem, where):
    return pltpu.make_async_remote_copy(
        src_ref=src,
        dst_ref=dst,
        send_sem=send_sem,
        recv_sem=recv_sem,
        device_id=where,
        device_id_type=MESH,
    )


def scan_rows(a, b, reverse):
    rows = a.shape[0]
    place = lax.broadcasted_iota(jnp.int32, a.shape, 0)
    step = 1
    while step < rows:
        if reverse:
            known = place < rows - step
            shift = rows - step
        else:
            known = place >= step
            shift = step
        a_far = jnp.where(known, pltpu.roll(a, shift, 0), 1.0)
        b_far = jnp.where(known, pltpu.roll(b, shift, 0), 0.0)
        b = a * b_far + b
        a = a * a_far
        step *= 2
    return a, b


def softplus_of_negative(w):
    t = jnp.exp(-jnp.abs(w))
    series = jnp.zeros_like(t)
    for k in range(10, 0, -1):
        series = t * ((1.0 / k if k % 2 else -1.0 / k) + series)
    return jnp.maximum(-w, 0.0) + jnp.where(t < 0.1, series, jnp.log(1.0 + t))


def one_minus_exp(y):
    series = jnp.ones_like(y)
    for k in range(10, 1, -1):
        series = 1.0 + y * (1.0 / k) * series
    return jnp.where(y > -0.5, -y * series, 1.0 - jnp.exp(y))


def block_kernel(
    n, m,
    nrm, cot, routes, probs, irms, gain, rin, rgate, igate, decay, extra, omat, gw, uw, dw,
    ggate, gup, gdown, gow, g_rec, g_dec, g_in,
    xo, co, rtv, pbv, irv, gnv, riv, rgv, igv, dcv, exv, omv, gwv, uwv, dwv,
    info, pos, wgt, keep, scin, admit, retain, cum, loc, prev, hid, carry, enters,
    xg, yg, act, dg, du, pr, stage, red, back, out, hid_all, mix_t, got,
    ld, zs, zr, xs, f1r, f2r, ds, dr, ns, nr, cs, cr, hs, hr, rs, rr, bs, br,
    gs, gr, ms, mr, es, er,
):
    me, j = lax.axis_index("sp"), lax.axis_index("tp")
    tok, feats = nrm.shape
    slots = pr.shape[0]
    cap, q = slots // n, feats // m
    chan, ff = keep.shape[1], gwv.shape[1]
    zn = n // 2
    z, par = lax.div(me, 2), lax.rem(me, 2)
    partner = me + 1 - 2 * par
    high, low = sides(m)
    upper, lower = lax.div(j, low), lax.rem(j, low)
    toks = lambda s: pl.ds(pl.multiple_of(s * tok, tok), tok)
    rows = lambda s: pl.ds(pl.multiple_of(s * cap, cap), cap)
    rows2 = lambda s: pl.ds(pl.multiple_of(s * 2 * cap, 2 * cap), 2 * cap)
    cols = lambda t: pl.ds(pl.multiple_of(t * q, q), q)
    arrays = ((0, xo), (1, co))

    def size(i):
        return low if i == 0 else high

    def near(i, along, across):
        up, down = (across, along) if i == 0 else (along, across)
        return lax.rem(upper + up, high) * low + lax.rem(lower + down, low)

    def source(k):
        fewer = jnp.minimum(z, zn - 1 - z)
        paired = k <= 2 * fewer
        d = jnp.where(paired, lax.div(k + 1, 2), k - fewer)
        odd = lax.rem(k, 2)
        down = jnp.where(paired, odd, jnp.where(z > zn - 1 - z, 1, 0))
        return z + d - 2 * d * down

    loads = [
        pltpu.make_async_copy(src, dst, ld.at[at])
        for at, (src, dst) in enumerate(
            (
                (nrm, xo.at[toks(me)]),
                (cot, co.at[toks(me)]),
                (routes, rtv),
                (probs, pbv),
                (rgate, rgv),
                (decay, dcv),
                (extra, exv),
                (igate, igv),
                (rin, riv),
                (gw.at[0], gwv),
                (uw.at[0], uwv),
                (dw.at[0], dwv),
                (omat, omv),
                (gain, gnv),
                (irms, irv),
            )
        )
    ]
    for c in loads:
        c.start()
    greet(n, m, me, j)
    loads[0].wait()
    loads[1].wait()

    def line(i, o, s, up):
        block = o.at[toks(2 * s + par), cols(j)]
        to = me + 2 if up else me - 2
        return send(block, block, zs.at[i, int(up), s], zr.at[i, s], {"sp": to})

    for i, o in arrays:
        @pl.when(z + 1 < zn)
        def _():
            line(i, o, z, True).start()

        @pl.when(z > 0)
        def _():
            line(i, o, z, False).start()

    def across(i, o, s):
        block = o.at[toks(2 * s + par)]
        return send(block, block, ds.at[i], dr.at[i, s], {"sp": partner})

    for i, o in arrays:
        across(i, o, z).start()

    loads[2].wait()
    loads[3].wait()
    info[me] = jnp.concatenate(
        [rtv[...].astype(F32), pbv[...], jnp.zeros((4, tok), F32)], axis=0
    )

    def told(k):
        to = lax.rem(me + k, n)
        return send(info.at[me], info.at[me], ns, nr.at[k], {"sp": to})

    def tell(k, _):
        told(k).start()
        return 0

    lax.fori_loop(1, n, tell, 0)

    for at in range(4, 9):
        loads[at].wait()
    speed = softplus_of_negative(dcv[...])
    retain[...] = jax.nn.sigmoid(rgv[...].astype(F32))
    admit[...] = jax.nn.sigmoid(igv[...].astype(F32))
    log_keep = -8.0 * retain[...] * speed + exv[...]
    keep[...] = jnp.exp(log_keep)
    scin[...] = jnp.sqrt(one_minus_exp(2.0 * log_keep))
    a, b = scan_rows(keep[...], scin[...] * admit[...] * riv[...].astype(F32), False)
    cum[...] = a
    loc[...] = b
    carry[me] = jnp.concatenate(
        [a[tok - 1 : tok], b[tok - 1 : tok], jnp.zeros((6, chan), F32)], axis=0
    )

    def carried(k):
        to = lax.rem(me + k, n)
        return send(carry.at[me], carry.at[me], cs, cr.at[k], {"sp": to})

    def start_carry(k, _):
        carried(k).start()
        return 0

    lax.fori_loop(1, n, start_carry, 0)

    earlier = (
        lax.broadcasted_iota(jnp.int32, (tok, tok), 0)
        < lax.broadcasted_iota(jnp.int32, (tok, tok), 1)
    ).astype(F32).astype(BF16)

    def place(k, _):
        s = lax.rem(me - k + n, n)

        @pl.when(k > 0)
        def _():
            send(info.at[s], info.at[s], ns, nr.at[k], {"sp": s}).wait_recv()

        mine = info[s]
        first, second = mine[0:1] == me.astype(F32), mine[1:2] == me.astype(F32)
        member = jnp.where(jnp.logical_or(first, second), 1.0, 0.0)
        wide = jnp.broadcast_to(member, (8, tok))
        ranking = jnp.dot(wide.astype(BF16), earlier, preferred_element_type=F32)
        pos[s] = jnp.where(wide > 0.0, ranking, -1.0)
        weight = jnp.where(first, mine[2:3], 0.0) + jnp.where(second, mine[3:4], 0.0)
        wgt[s] = jnp.broadcast_to(weight, (8, tok))
        return 0

    lax.fori_loop(0, n, place, 0)
    for at in range(9, 15):
        loads[at].wait()

    def onward(s, i, o):
        block = o.at[toks(2 * s + par), cols(j)]
        for p in range(1, size(i)):
            send(block, block, xs.at[i], f1r.at[i, s], {"tp": near(i, p, 0)}).start()
        for p in range(1, size(1 - i)):
            send(block, block, xs.at[i], f2r.at[i, s], {"tp": near(i, 0, p)}).start()

    def several(o, s, count):
        return o.at[toks(2 * s + par), pl.ds(0, count * q)]

    def relayed(s):
        for i, o in arrays:
            if size(i) > 1:
                part = several(o, s, size(i) - 1)
                send(part, part, xs.at[i], f1r.at[i, s], {"tp": near(i, 1, 0)}).wait_recv()
            for c in range(1, size(i)):
                block = o.at[toks(2 * s + par), cols(near(i, size(i) - c, 0))]
                for p in range(1, size(1 - i)):
                    send(block, block, xs.at[i], f2r.at[i, s], {"tp": near(i, 0, p)}).start()

    def whole(s):
        for i, o in arrays:
            if size(1 - i) > 1:
                part = several(o, s, m - size(i))
                send(part, part, xs.at[i], f2r.at[i, s], {"tp": near(i, 0, 1)}).wait_recv()
            across(i, o, s).start()

    span = min(feats, 512)
    unit = min(ff, 256)

    def compute(s):
        other = 2 * s + 1 - par
        for i, o in arrays:
            block = o.at[toks(other)]
            send(block, block, ds.at[i], dr.at[i, s], {"sp": partner}).wait_recv()
        low_at, high_at = pos[2 * s][0:1], pos[2 * s + 1][0:1]
        high_at = jnp.where(high_at >= 0.0, high_at + float(cap), -1.0)
        at = jnp.concatenate([low_at, high_at], axis=1)
        weight = jnp.concatenate([wgt[2 * s][0:1], wgt[2 * s + 1][0:1]], axis=1)
        here = lax.broadcasted_iota(jnp.int32, (2 * cap, 2 * tok), 0).astype(F32)
        hit = here == at
        one = jnp.where(hit, 1.0, 0.0)
        share = jnp.sum(jnp.where(hit, weight, 0.0), axis=1, keepdims=True)
        one = one.astype(BF16)
        pair = pl.ds(pl.multiple_of(s * 2 * tok, 2 * tok), 2 * tok)
        land = rows2(s)
        for t in range(feats // span):
            f = pl.ds(t * span, span)
            xg[land, f] = jnp.dot(one, xo[pair, f], preferred_element_type=F32).astype(BF16)
            yg[land, f] = (share * jnp.dot(one, co[pair, f], preferred_element_type=F32)).astype(
                BF16
            )
        for t in range(ff // unit):
            f = pl.ds(t * unit, unit)
            gate = jnp.dot(xg[land, :], gwv[:, f], preferred_element_type=F32)
            up = jnp.dot(xg[land, :], uwv[:, f], preferred_element_type=F32)
            d_act = lax.dot_general(yg[land, :], dwv[f, :], COLDIMS, preferred_element_type=F32)
            sigma = jax.nn.sigmoid(gate)
            swish = gate * sigma
            act[land, f] = (swish * up).astype(BF16)
            dg[land, f] = (d_act * up * sigma * (1.0 + gate * (1.0 - sigma))).astype(BF16)
            du[land, f] = (d_act * swish).astype(BF16)
        for t in range(feats // span):
            f = pl.ds(t * span, span)
            part = lax.dot_general(dg[land, :], gwv[f, :], COLDIMS, preferred_element_type=F32)
            part += lax.dot_general(du[land, :], uwv[f, :], COLDIMS, preferred_element_type=F32)
            pr[land, f] = part.astype(BF16)
        for p in range(1, m):
            far = lax.rem(j + p, m)
            send(
                pr.at[land, cols(far)], stage.at[p - 1, land], rs.at[s], rr.at[s], {"tp": far}
            ).start()

    def shipped(s):
        return send(red.at[rows(s)], back.at[rows(me)], bs, br.at[me], {"sp": s})

    def reduce(s):
        land = rows2(s)
        block = stage.at[:, land]
        arrived = send(block, block, rs.at[s], rr.at[s], {"tp": lax.rem(j + 1, m)})
        arrived.wait_recv()
        arrived.wait_send()
        total = pr[land, cols(j)].astype(F32)
        for p in range(1, m):
            total = total + stage[p - 1, land].astype(F32)
        red[land] = total.astype(BF16)
        for c in range(2):
            @pl.when(2 * s + c != me)
            def _():
                shipped(2 * s + c).start()

    def step(k, _):
        @pl.when(k < zn)
        def _():
            s = source(k)
            for i, o in arrays:
                line(i, o, s, True).wait_recv()

                @pl.when(jnp.logical_and(s < z, z + 1 < zn))
                def _():
                    line(i, o, s, True).start()

                @pl.when(jnp.logical_and(s > z, z > 0))
                def _():
                    line(i, o, s, False).start()

                onward(s, i, o)

        @pl.when(jnp.logical_and(k >= 2, k < zn + 1))
        def _():
            relayed(source(k - 1))

        @pl.when(k >= 3)
        def _():
            whole(source(k - 2))

        @pl.when(jnp.logical_or(k == 1, k >= 3))
        def _():
            compute(source(jnp.where(k == 1, 0, k - 2)))

        @pl.when(k >= 3)
        def _():
            reduce(source(k - 3))

        return 0

    lax.fori_loop(1, zn + 2, step, 0)

    def take_carry(k, _):
        s = lax.rem(me - k + n, n)
        send(carry.at[s], carry.at[s], cs, cr.at[k], {"sp": s}).wait_recv()
        return 0

    lax.fori_loop(1, n, take_carry, 0)
    state = jnp.zeros((1, chan), F32)
    for s in range(n):
        state = jnp.where(s < me, carry[s, 0:1] * state + carry[s, 1:2], state)
    states = loc[...] + cum[...] * state
    hid[...] = states.astype(BF16)
    spot = lax.broadcasted_iota(jnp.int32, (tok, chan), 0)
    prev[...] = jnp.where(spot >= 1, pltpu.roll(states, 1, 0), state)
    hid_all[me] = hid[...]

    def shared(k):
        to = lax.rem(me + k, n)
        return send(hid, hid_all.at[me], hs, hr.at[k], {"sp": to})

    def share_hidden(k, _):
        shared(k).start()
        return 0

    lax.fori_loop(1, n, share_hidden, 0)

    def wide_grads(t, _):
        f = pl.ds(pl.multiple_of(t * 256, 256), 256)
        rowsof = xg[:, f]
        ggate[0, f, :] = lax.dot_general(
            rowsof, dg[...], ROWDIMS, preferred_element_type=F32
        ).astype(BF16)
        gup[0, f, :] = lax.dot_general(
            rowsof, du[...], ROWDIMS, preferred_element_type=F32
        ).astype(BF16)
        return 0

    lax.fori_loop(0, feats // 256, wide_grads, 0)
    for t in range(ff // min(ff, 128)):
        f = pl.ds(t * min(ff, 128), min(ff, 128))
        gdown[0, f, :] = lax.dot_general(
            act[:, f], yg[...], ROWDIMS, preferred_element_type=F32
        ).astype(BF16)

    reduce(source(zn - 1))
    back[rows(me)] = red[rows(me)]

    own = info[me]
    experts = lax.broadcasted_iota(jnp.int32, (n, tok), 0).astype(F32)
    member = jnp.where(jnp.logical_or(own[0:1] == experts, own[1:2] == experts), 1.0, 0.0)
    ranking = jnp.dot(member.astype(BF16), earlier, preferred_element_type=F32)
    ranking = jnp.where(member > 0.0, ranking, -1.0)
    depth = lax.broadcasted_iota(jnp.int32, (n, cap, tok), 1).astype(F32)
    pick = jnp.where(depth == ranking[:, None, :], 1.0, 0.0).reshape(slots, tok).astype(BF16)

    def collect(k, _):
        s = lax.rem(me - k + n, n)
        block = back.at[rows(s)]
        send(block, block, bs, br.at[s], {"sp": s}).wait_recv()
        return 0

    lax.fori_loop(1, n, collect, 0)
    total = lax.dot_general(pick, back[...], ROWDIMS, preferred_element_type=F32)
    out[:, cols(j)] = total.astype(BF16)
    mine = out.at[:, cols(j)]
    for p in range(1, m):
        send(mine, mine, gs.at[p], gr.at[p], {"tp": lax.rem(j + p, m)}).start()
    for p in range(1, m):
        far = lax.rem(j - p + m, m)
        theirs = out.at[:, cols(far)]
        send(mine, mine, gs.at[p], gr.at[p], {"tp": far}).wait_send()
        send(theirs, theirs, gs.at[p], gr.at[p], {"tp": far}).wait_recv()

    slab = feats // n
    slabs = lambda s: pl.ds(pl.multiple_of(s * slab, slab), slab)
    scale = gnv[...]
    nhat = xo[toks(me)].astype(F32) / scale
    gained = scale * out[...].astype(F32)
    stat = jnp.mean(gained * nhat, axis=1, keepdims=True)
    root = jnp.broadcast_to(irv[...], (8, tok)).T[:, 0:1]
    mixed = co[toks(me)].astype(F32) + root * (gained - nhat * stat)
    mix_t[...] = mixed.T.astype(BF16)

    def blocks(k):
        to = lax.rem(me + k, n)
        return send(mix_t.at[slabs(to)], got.at[me], ms, mr.at[k], {"sp": to})

    def start_blocks(k, _):
        blocks(k).start()
        return 0

    lax.fori_loop(1, n, start_blocks, 0)
    d_state = jnp.dot(mixed.astype(BF16), omv[...], preferred_element_type=F32)
    here = keep[...]
    after = jnp.where(spot < tok - 1, pltpu.roll(here, tok - 1, 0), 1.0)
    a, b = scan_rows(after, d_state, True)
    enters[me] = jnp.broadcast_to(here[0:1] * b[0:1], (8, chan))
    cum[...] = a
    loc[...] = b

    def entering(k):
        to = lax.rem(me + k, n)
        return send(enters.at[me], enters.at[me], es, er.at[k], {"sp": to})

    def start_enter(k, _):
        entering(k).start()
        return 0

    lax.fori_loop(1, n, start_enter, 0)
    gow[...] = jnp.dot(mix_t[slabs(me)], hid_all[me], preferred_element_type=F32)

    def take_hidden(k, _):
        s = lax.rem(me - k + n, n)
        send(hid, hid_all.at[s], hs, hr.at[k], {"sp": s}).wait_recv()
        return 0

    lax.fori_loop(1, n, take_hidden, 0)

    def add(k, _):
        s = lax.rem(me - k + n, n)
        send(got.at[s], got.at[s], ms, mr.at[k], {"sp": s}).wait_recv()
        gow[...] += jnp.dot(got[s], hid_all[s], preferred_element_type=F32)
        return 0

    lax.fori_loop(1, n, add, 0)

    def take_enter(k, _):
        s = lax.rem(me - k + n, n)
        send(enters.at[s], enters.at[s], es, er.at[k], {"sp": s}).wait_recv()
        return 0

    lax.fori_loop(1, n, take_enter, 0)
    enter = jnp.zeros((1, chan), F32)
    for s in range(n - 1, -1, -1):
        enter = jnp.where(s > me, carry[s, 0:1] * enter + enters[s, 0:1], enter)
    total = loc[...] + cum[...] * enter
    inward, opened, held, kept = scin[...], admit[...], retain[...], keep[...]
    signal = riv[...].astype(F32)
    g_rec[...] = total * inward * opened
    g_in[...] = total * inward * signal * opened * (1.0 - opened)
    d_log = total * prev[...] * kept - total * opened * signal * kept * kept / inward
    g_dec[...] = d_log * (-8.0 * speed) * held * (1.0 - held)

    def flush(s, _):
        for i, o in arrays:
            @pl.when(jnp.logical_and(s <= z, z + 1 < zn))
            def _():
                line(i, o, s, True).wait_send()

            @pl.when(jnp.logical_and(s >= z, z > 0))
            def _():
                line(i, o, s, False).wait_send()

        return 0

    lax.fori_loop(0, zn, flush, 0)
    for i, o in arrays:
        part = o.at[pl.ds(0, (zn - 1) * tok), pl.ds(0, (m - 1) * q)]
        send(part, part, xs.at[i], f1r.at[i, 0], {"tp": lax.rem(j + 1, m)}).wait_send()
        part = o.at[pl.ds(0, zn * tok)]
        send(part, part, ds.at[i], dr.at[i, 0], {"sp": partner}).wait_send()
    to = {"sp": partner}
    others = pl.ds(0, n - 1)
    send(info.at[others], info.at[others], ns, nr.at[0], to).wait_send()
    send(carry.at[others], carry.at[others], cs, cr.at[0], to).wait_send()
    send(enters.at[others], enters.at[others], es, er.at[0], to).wait_send()
    send(hid_all.at[others], hid_all.at[others], hs, hr.at[0], to).wait_send()
    send(got.at[others], got.at[others], ms, mr.at[0], to).wait_send()
    part = red.at[pl.ds(0, (n - 1) * cap)]
    send(part, part, bs, br.at[0], to).wait_send()


def shards(
    cotangent,
    normed,
    inverse_root_mean_square,
    expert_norm_scale,
    routes,
    route_probability_weight,
    gate_weight,
    up_weight,
    down_weight,
    recurrence_input,
    recurrence_gate_logits,
    input_gate_logits,
    channel_decay_weight,
    extra_log_decay,
    output_matrix,
):
    tok, feats = normed.shape
    n, m = lax.axis_size("sp"), lax.axis_size("tp")
    picks = routes.shape[1]
    cap = 2 * picks * tok // n
    slots = n * cap
    q = feats // m
    ff = gate_weight.shape[2]
    chan = recurrence_input.shape[1]
    zn = n // 2
    dma = pltpu.SemaphoreType.DMA
    vmem = lambda *s: pltpu.VMEM(s, F32)
    half = lambda *s: pltpu.VMEM(s, BF16)
    outs = [
        ((1, feats, ff), BF16),
        ((1, feats, ff), BF16),
        ((1, ff, feats), BF16),
        ((feats // n, chan), F32),
        ((tok, chan), F32),
        ((tok, chan), F32),
        ((tok, chan), F32),
    ]
    scratch = [
        half(n * tok, feats),
        half(n * tok, feats),
        pltpu.VMEM((picks, tok), jnp.int32),
        vmem(picks, tok),
        vmem(1, tok),
        vmem(1, feats),
        half(tok, chan),
        half(tok, chan),
        half(tok, chan),
        vmem(1, chan),
        vmem(tok, chan),
        half(feats, chan),
        half(feats, ff),
        half(feats, ff),
        half(ff, feats),
        vmem(n, 8, tok),
        vmem(n, 8, tok),
        vmem(n, 8, tok),
        vmem(tok, chan),
        vmem(tok, chan),
        vmem(tok, chan),
        vmem(tok, chan),
        vmem(tok, chan),
        vmem(tok, chan),
        vmem(tok, chan),
        half(tok, chan),
        vmem(n, 8, chan),
        vmem(n, 8, chan),
        half(slots, feats),
        half(slots, feats),
        half(slots, ff),
        half(slots, ff),
        half(slots, ff),
        half(slots, feats),
        half(m - 1, slots, q),
        half(slots, q),
        half(slots, q),
        half(tok, feats),
        half(n, tok, chan),
        half(feats, tok),
        half(n, feats // n, tok),
        dma((15,)),
        dma((2, 2, zn)),
        dma((2, zn)),
        dma((2,)),
        dma((2, zn)),
        dma((2, zn)),
        dma((2,)),
        dma((2, zn)),
        dma,
        dma((n,)),
        dma,
        dma((n,)),
        dma,
        dma((n,)),
        dma((zn,)),
        dma((zn,)),
        dma,
        dma((n,)),
        dma((m,)),
        dma((m,)),
        dma,
        dma((n,)),
        dma,
        dma((n,)),
    ]
    args = (
        normed,
        cotangent,
        routes.T,
        route_probability_weight.T,
        inverse_root_mean_square[None, :],
        expert_norm_scale[None, :],
        recurrence_input,
        recurrence_gate_logits,
        input_gate_logits,
        channel_decay_weight[None, :],
        extra_log_decay,
        output_matrix,
        gate_weight,
        up_weight,
        down_weight,
    )
    return pl.pallas_call(
        functools.partial(block_kernel, n, m),
        out_shape=tuple(jax.ShapeDtypeStruct(s, d) for s, d in outs),
        in_specs=[pl.BlockSpec(memory_space=pl.ANY)] * len(args),
        out_specs=tuple(pl.BlockSpec(memory_space=pltpu.VMEM) for _ in outs),
        scratch_shapes=scratch,
        compiler_params=pltpu.CompilerParams(
            collective_id=0, has_side_effects=True, vmem_limit_bytes=VMEM_LIMIT
        ),
    )(*args)


def solution(mesh):
    return jax.shard_map(
        shards,
        mesh=mesh,
        in_specs=(
            P("sp", None),
            P("sp", None),
            P("sp"),
            P(),
            P("sp", None),
            P("sp", None),
            P("sp", None, "tp"),
            P("sp", None, "tp"),
            P("sp", "tp", None),
            P("sp", "tp"),
            P("sp", "tp"),
            P("sp", "tp"),
            P("tp"),
            P("sp", "tp"),
            P(None, "tp"),
        ),
        out_specs=(
            P("sp", None, "tp"),
            P("sp", None, "tp"),
            P("sp", "tp", None),
            P("sp", "tp"),
            P("sp", "tp"),
            P("sp", "tp"),
            P("sp", "tp"),
        ),
        check_vma=False,
    )
```

time: 145 us -> 119 us (0.82)
  matrix products: 22 us -> 0 us
  other arithmetic: 6.11 us -> 0 us
  local copies, waits for them, and re-layouts: 5.43 us -> 9.55 us
  Pallas kernels: 111 us -> 109 us
    dot_general x11 -> x0, matrix products: 22 us -> none  [the longest x1 2.99 us: shards(): gate_pre = jnp.dot(token_recv, gate_w, preferred_element_type=f32)]
    unnamed x24 -> x19, local copies, waits for them, and re-layouts: 3.59 us -> 9.55 us
    mul x3 -> x0, other arithmetic: 4.41 us -> none  [the longest x1 1.88 us: shards(): grad_input_gate = total * scale_in * signal * admit * (1.0 - admit)]
    pallas_call x2 -> x1, Pallas kernels: 111 us -> 109 us  [shards(): pl.pallas_call(functools.partial(block_kernel, n, m), out_shape=tuple((ja...]
    broadcast_in_dim x2 -> x0, local copies, waits for them, and re-layouts: 1.5 us -> none  [the longest x1 0.76 us: shards(): jnp.where(h, route_probability_weight[:, k][None, :], 0.0)]
where the time goes in v1:
time: 119 us
  Pallas kernels  109 us (92%)
  local copies, waits for them, and re-layouts  9.55 us (8%)
    pallas_call x1, Pallas kernels, shards(): pl.pallas_call(functools.partial(block_kernel, n, m), out_shape=tuple((ja...  109 us
    unnamed x19, local copies, waits for them, and re-layouts  9.55 us

profile of v1, /device:TPU:0, one launch (start us, length us, event | category | flops | bytes accessed | tf_op | source)
XLA Modules:
  0.0 118.8 jit_solution(2348610278745477987)
XLA Ops:
  0.6 108.6 %shard_map.198 = (bf16[1,2048,512]{2,1,0:T(8,128)(2,1)}, bf16[1,2048,512]{2,1,0:T(8,128)(2,1)}, bf16[1,512,2048]{2,1,0:T(8,128)(2,1)}, f32[256,256]{1,0:T(8,128)...) custom-call(bf16[128,2048]{1,0:T(8,128)(2,1)} %nrm.1, bf16[128,2048]{1,0:T(8,128)(2,1)} %cot.1, ...), custom_call_target="tpu_custom_call" | custom-call | tf_op jit(solution)/shard_map/pallas_call | solution.py:658
  109.2 0.0 copy-start.1
  109.2 3.2 %copy.29 = bf16[1,2048,512]{2,1,0:T(8,128)(2,1)} copy(bf16[1,2048,512]{2,1,0:T(8,128)(2,1)} %get-tuple-element.14) | data formatting | bytes 4194304
  112.4 0.0 copy-done.1
  112.4 0.0 copy-start
  112.4 1.3 %copy.30 = bf16[1,2048,512]{2,1,0:T(8,128)(2,1)} copy(bf16[1,2048,512]{2,1,0:T(8,128)(2,1)S(1)} %copy-done.1) | data formatting | bytes 4194304
  113.7 1.0 copy-done
  114.8 0.0 copy-start.2
  114.8 0.0 copy-start.5
  114.8 0.0 copy-start.4
  114.8 0.0 copy-start.3
  114.8 1.3 %copy.31 = bf16[1,512,2048]{2,1,0:T(8,128)(2,1)} copy(bf16[1,512,2048]{2,1,0:T(8,128)(2,1)S(1)} %copy-done) | data formatting | bytes 4194304
  116.1 0.0 copy-done.2
  116.1 0.7 copy.32
  116.8 0.0 copy-done.5
  116.8 0.7 copy.33
  117.5 0.0 copy-done.4
  117.5 0.7 copy.34
  118.1 0.0 copy-done.3
  118.1 0.7 copy.35
Async XLA Ops:
  109.2 3.2 %copy-start.1 = (bf16[1,2048,512]{2,1,0:T(8,128)(2,1)S(1)}, bf16[1,2048,512]{2,1,0:T(8,128)(2,1)}, u32[]{:S(2)}) copy-start(bf16[1,2048,512]{2,1,0:T(8,128)(2,1)} %get-tuple-element.15) | copy-start | bytes 6291460
  112.4 2.3 %copy-start = (bf16[1,512,2048]{2,1,0:T(8,128)(2,1)S(1)}, bf16[1,512,2048]{2,1,0:T(8,128)(2,1)}, u32[]{:S(2)}) copy-start(bf16[1,512,2048]{2,1,0:T(8,128)(2,1)} %get-tuple-element.16) | copy-start | bytes 6291460
  114.8 1.3 %copy-start.2 = (f32[256,256]{1,0:T(8,128)S(1)}, f32[256,256]{1,0:T(8,128)}, u32[]{:S(2)}) copy-start(f32[256,256]{1,0:T(8,128)} %get-tuple-element.17) | copy-start | bytes 786436
  114.8 2.0 %copy-start.5 = (f32[128,256]{1,0:T(8,128)S(1)}, f32[128,256]{1,0:T(8,128)}, u32[]{:S(2)}) copy-start(f32[128,256]{1,0:T(8,128)} %get-tuple-element.18) | copy-start | bytes 393220
  114.8 2.7 %copy-start.4 = (f32[128,256]{1,0:T(8,128)S(1)}, f32[128,256]{1,0:T(8,128)}, u32[]{:S(2)}) copy-start(f32[128,256]{1,0:T(8,128)} %get-tuple-element.19) | copy-start | bytes 393220
  114.8 3.4 %copy-start.3 = (f32[128,256]{1,0:T(8,128)S(1)}, f32[128,256]{1,0:T(8,128)}, u32[]{:S(2)}) copy-start(f32[128,256]{1,0:T(8,128)} %get-tuple-element.20) | copy-start | bytes 393220

commit v2 on v1

--- a/solution.py
+++ b/solution.py
@@ -9,6 +9,8 @@
 
 MESH = pl.DeviceIdType.MESH
 VMEM_LIMIT = 63 * 1024 * 1024
+SPARE = 8 * 1024 * 1024
+LEAST = 12 * 1024 * 1024
 F32, BF16 = jnp.float32, jnp.bfloat16
 ROWDIMS = (((0,), (0,)), ((), ()))
 COLDIMS = (((1,), (1,)), ((), ()))
@@ -82,7 +84,7 @@
     nrm, cot, routes, probs, irms, gain, rin, rgate, igate, decay, extra, omat, gw, uw, dw,
     ggate, gup, gdown, gow, g_rec, g_dec, g_in,
     xo, co, rtv, pbv, irv, gnv, riv, rgv, igv, dcv, exv, omv, gwv, uwv, dwv,
-    info, pos, wgt, keep, scin, admit, retain, cum, loc, prev, hid, carry, enters,
+    info, keep, scin, admit, retain, cum, loc, prev, hid, carry, enters,
     xg, yg, act, dg, du, pr, stage, red, back, out, hid_all, mix_t, got,
     ld, zs, zr, xs, f1r, f2r, ds, dr, ns, nr, cs, cr, hs, hr, rs, rr, bs, br,
     gs, gr, ms, mr, es, er,
@@ -122,10 +124,10 @@
         pltpu.make_async_copy(src, dst, ld.at[at])
         for at, (src, dst) in enumerate(
             (
+                (routes, rtv),
+                (probs, pbv),
                 (nrm, xo.at[toks(me)]),
                 (cot, co.at[toks(me)]),
-                (routes, rtv),
-                (probs, pbv),
                 (rgate, rgv),
                 (decay, dcv),
                 (extra, exv),
@@ -145,6 +147,22 @@
     greet(n, m, me, j)
     loads[0].wait()
     loads[1].wait()
+    info[me] = jnp.concatenate(
+        [rtv[...].astype(F32), pbv[...], jnp.zeros((4, tok), F32)], axis=0
+    )
+
+    def told(k):
+        to = lax.rem(me + k, n)
+        return send(info.at[me], info.at[me], ns, nr.at[me], {"sp": to})
+
+    def tell(k, _):
+        told(k).start()
+        return 0
+
+    lax.fori_loop(1, n, tell, 0)
+
+    loads[2].wait()
+    loads[3].wait()
 
     def line(i, o, s, up):
         block = o.at[toks(2 * s + par), cols(j)]
@@ -166,22 +184,6 @@
 
     for i, o in arrays:
         across(i, o, z).start()
-
-    loads[2].wait()
-    loads[3].wait()
-    info[me] = jnp.concatenate(
-        [rtv[...].astype(F32), pbv[...], jnp.zeros((4, tok), F32)], axis=0
-    )
-
-    def told(k):
-        to = lax.rem(me + k, n)
-        return send(info.at[me], info.at[me], ns, nr.at[k], {"sp": to})
-
-    def tell(k, _):
-        told(k).start()
-        return 0
-
-    lax.fori_loop(1, n, tell, 0)
 
     for at in range(4, 9):
         loads[at].wait()
@@ -213,24 +215,19 @@
         < lax.broadcasted_iota(jnp.int32, (tok, tok), 1)
     ).astype(F32).astype(BF16)
 
-    def place(k, _):
-        s = lax.rem(me - k + n, n)
-
-        @pl.when(k > 0)
-        def _():
-            send(info.at[s], info.at[s], ns, nr.at[k], {"sp": s}).wait_recv()
+    def place(s):
+        @pl.when(s != me)
+        def _():
+            send(info.at[s], info.at[s], ns, nr.at[s], {"sp": s}).wait_recv()
 
         mine = info[s]
         first, second = mine[0:1] == me.astype(F32), mine[1:2] == me.astype(F32)
         member = jnp.where(jnp.logical_or(first, second), 1.0, 0.0)
         wide = jnp.broadcast_to(member, (8, tok))
         ranking = jnp.dot(wide.astype(BF16), earlier, preferred_element_type=F32)
-        pos[s] = jnp.where(wide > 0.0, ranking, -1.0)
         weight = jnp.where(first, mine[2:3], 0.0) + jnp.where(second, mine[3:4], 0.0)
-        wgt[s] = jnp.broadcast_to(weight, (8, tok))
-        return 0
-
-    lax.fori_loop(0, n, place, 0)
+        return jnp.where(member > 0.0, ranking[0:1], -1.0), weight
+
     for at in range(9, 15):
         loads[at].wait()
 
@@ -269,10 +266,10 @@
         for i, o in arrays:
             block = o.at[toks(other)]
             send(block, block, ds.at[i], dr.at[i, s], {"sp": partner}).wait_recv()
-        low_at, high_at = pos[2 * s][0:1], pos[2 * s + 1][0:1]
+        (low_at, low_weight), (high_at, high_weight) = place(2 * s), place(2 * s + 1)
         high_at = jnp.where(high_at >= 0.0, high_at + float(cap), -1.0)
         at = jnp.concatenate([low_at, high_at], axis=1)
-        weight = jnp.concatenate([wgt[2 * s][0:1], wgt[2 * s + 1][0:1]], axis=1)
+        weight = jnp.concatenate([low_weight, high_weight], axis=1)
         here = lax.broadcasted_iota(jnp.int32, (2 * cap, 2 * tok), 0).astype(F32)
         hit = here == at
         one = jnp.where(hit, 1.0, 0.0)
@@ -325,8 +322,35 @@
             def _():
                 shipped(2 * s + c).start()
 
+    spot = lax.broadcasted_iota(jnp.int32, (tok, chan), 0)
+
+    def hidden():
+        def take_carry(k, _):
+            s = lax.rem(me - k + n, n)
+            send(carry.at[s], carry.at[s], cs, cr.at[k], {"sp": s}).wait_recv()
+            return 0
+
+        lax.fori_loop(1, n, take_carry, 0)
+        state = jnp.zeros((1, chan), F32)
+        for s in range(n):
+            state = jnp.where(s < me, carry[s, 0:1] * state + carry[s, 1:2], state)
+        states = loc[...] + cum[...] * state
+        hid[...] = states.astype(BF16)
+        prev[...] = jnp.where(spot >= 1, pltpu.roll(states, 1, 0), state)
+        hid_all[me] = hid[...]
+
+        def shared(k):
+            to = lax.rem(me + k, n)
+            return send(hid, hid_all.at[me], hs, hr.at[k], {"sp": to})
+
+        def share_hidden(k, _):
+            shared(k).start()
+            return 0
+
+        lax.fori_loop(1, n, share_hidden, 0)
+
     def step(k, _):
-        @pl.when(k < zn)
+        @pl.when(jnp.logical_and(k >= 1, k < zn))
         def _():
             s = source(k)
             for i, o in arrays:
@@ -342,6 +366,10 @@
 
                 onward(s, i, o)
 
+        @pl.when(k == zn - 1)
+        def _():
+            hidden()
+
         @pl.when(jnp.logical_and(k >= 2, k < zn + 1))
         def _():
             relayed(source(k - 1))
@@ -350,9 +378,9 @@
         def _():
             whole(source(k - 2))
 
-        @pl.when(jnp.logical_or(k == 1, k >= 3))
-        def _():
-            compute(source(jnp.where(k == 1, 0, k - 2)))
+        @pl.when(jnp.logical_or(k == 0, k >= 3))
+        def _():
+            compute(source(jnp.where(k == 0, 0, k - 2)))
 
         @pl.when(k >= 3)
         def _():
@@ -360,32 +388,7 @@
 
         return 0
 
-    lax.fori_loop(1, zn + 2, step, 0)
-
-    def take_carry(k, _):
-        s = lax.rem(me - k + n, n)
-        send(carry.at[s], carry.at[s], cs, cr.at[k], {"sp": s}).wait_recv()
-        return 0
-
-    lax.fori_loop(1, n, take_carry, 0)
-    state = jnp.zeros((1, chan), F32)
-    for s in range(n):
-        state = jnp.where(s < me, carry[s, 0:1] * state + carry[s, 1:2], state)
-    states = loc[...] + cum[...] * state
-    hid[...] = states.astype(BF16)
-    spot = lax.broadcasted_iota(jnp.int32, (tok, chan), 0)
-    prev[...] = jnp.where(spot >= 1, pltpu.roll(states, 1, 0), state)
-    hid_all[me] = hid[...]
-
-    def shared(k):
-        to = lax.rem(me + k, n)
-        return send(hid, hid_all.at[me], hs, hr.at[k], {"sp": to})
-
-    def share_hidden(k, _):
-        shared(k).start()
-        return 0
-
-    lax.fori_loop(1, n, share_hidden, 0)
+    lax.fori_loop(0, zn + 2, step, 0)
 
     def wide_grads(t, _):
         f = pl.ds(pl.multiple_of(t * 256, 256), 256)
@@ -452,7 +455,6 @@
         blocks(k).start()
         return 0
 
-    lax.fori_loop(1, n, start_blocks, 0)
     d_state = jnp.dot(mixed.astype(BF16), omv[...], preferred_element_type=F32)
     here = keep[...]
     after = jnp.where(spot < tok - 1, pltpu.roll(here, tok - 1, 0), 1.0)
@@ -470,22 +472,13 @@
         return 0
 
     lax.fori_loop(1, n, start_enter, 0)
+    lax.fori_loop(1, n, start_blocks, 0)
     gow[...] = jnp.dot(mix_t[slabs(me)], hid_all[me], preferred_element_type=F32)
 
     def take_hidden(k, _):
         s = lax.rem(me - k + n, n)
         send(hid, hid_all.at[s], hs, hr.at[k], {"sp": s}).wait_recv()
         return 0
-
-    lax.fori_loop(1, n, take_hidden, 0)
-
-    def add(k, _):
-        s = lax.rem(me - k + n, n)
-        send(got.at[s], got.at[s], ms, mr.at[k], {"sp": s}).wait_recv()
-        gow[...] += jnp.dot(got[s], hid_all[s], preferred_element_type=F32)
-        return 0
-
-    lax.fori_loop(1, n, add, 0)
 
     def take_enter(k, _):
         s = lax.rem(me - k + n, n)
@@ -503,6 +496,16 @@
     g_in[...] = total * inward * signal * opened * (1.0 - opened)
     d_log = total * prev[...] * kept - total * opened * signal * kept * kept / inward
     g_dec[...] = d_log * (-8.0 * speed) * held * (1.0 - held)
+
+    lax.fori_loop(1, n, take_hidden, 0)
+
+    def add(k, _):
+        s = lax.rem(me - k + n, n)
+        send(got.at[s], got.at[s], ms, mr.at[k], {"sp": s}).wait_recv()
+        gow[...] += jnp.dot(got[s], hid_all[s], preferred_element_type=F32)
+        return 0
+
+    lax.fori_loop(1, n, add, 0)
 
     def flush(s, _):
         for i, o in arrays:
@@ -531,6 +534,29 @@
     send(got.at[others], got.at[others], ms, mr.at[0], to).wait_send()
     part = red.at[pl.ds(0, (n - 1) * cap)]
     send(part, part, bs, br.at[0], to).wait_send()
+
+
+def place_kernel(*refs):
+    count = len(refs) // 2
+    sems = refs[-1]
+    copies = [
+        pltpu.make_async_copy(refs[at], refs[count + at], sems.at[at]) for at in range(count)
+    ]
+    for c in copies:
+        c.start()
+    for c in copies:
+        c.wait()
+
+
+def vmem_limit(outs, scratch):
+    total = 0
+    held = [(s.shape, s.dtype) for s in scratch if s.dtype in (F32, BF16, jnp.int32)]
+    for shape, kind in list(outs) + held:
+        size = -(-shape[-1] // 128) * 128 * -(-shape[-2] // 8) * 8 * jnp.dtype(kind).itemsize
+        for d in shape[:-2]:
+            size *= d
+        total += size
+    return min(VMEM_LIMIT, total + SPARE)
 
 
 def shards(
@@ -587,8 +613,6 @@
         half(feats, ff),
         half(feats, ff),
         half(ff, feats),
-        vmem(n, 8, tok),
-        vmem(n, 8, tok),
         vmem(n, 8, tok),
         vmem(tok, chan),
         vmem(tok, chan),
@@ -655,16 +679,25 @@
         up_weight,
         down_weight,
     )
-    return pl.pallas_call(
+    args = [pltpu.with_memory_space_constraint(a, pltpu.HBM) for a in args]
+    results = pl.pallas_call(
         functools.partial(block_kernel, n, m),
         out_shape=tuple(jax.ShapeDtypeStruct(s, d) for s, d in outs),
-        in_specs=[pl.BlockSpec(memory_space=pl.ANY)] * len(args),
+        in_specs=[pl.BlockSpec(memory_space=pltpu.HBM)] * len(args),
         out_specs=tuple(pl.BlockSpec(memory_space=pltpu.VMEM) for _ in outs),
         scratch_shapes=scratch,
         compiler_params=pltpu.CompilerParams(
-            collective_id=0, has_side_effects=True, vmem_limit_bytes=VMEM_LIMIT
+            collective_id=0, has_side_effects=True, vmem_limit_bytes=vmem_limit(outs, scratch)
         ),
     )(*args)
+    return pl.pallas_call(
+        place_kernel,
+        out_shape=tuple(jax.ShapeDtypeStruct(s, d) for s, d in outs),
+        in_specs=[pl.BlockSpec(memory_space=pltpu.VMEM)] * len(outs),
+        out_specs=tuple(pl.BlockSpec(memory_space=pltpu.HBM) for _ in outs),
+        scratch_shapes=[dma((len(outs),))],
+        compiler_params=pltpu.CompilerParams(vmem_limit_bytes=LEAST),
+    )(*results)
 
 
 def solution(mesh):

time: 119 us -> 94.5 us (0.79)
  Pallas kernels: 109 us -> 93.7 us
  local copies, waits for them, and re-layouts: 9.55 us -> 0 us
    pallas_call x1, Pallas kernels: 109 us -> 90.8 us  [shards(): pl.pallas_call(functools.partial(block_kernel, n, m), out_shape=tuple((ja...]
    unnamed x19 -> x0, local copies, waits for them, and re-layouts: 9.55 us -> none
    pallas_call x0 -> x1, Pallas kernels: none -> 2.89 us  [shards(): pl.pallas_call(place_kernel, out_shape=tuple((jax.ShapeDtypeStruct(s, d)...]
where the time goes in v2:
time: 94.5 us; the launch traced here: 94.3 us
  Pallas kernels  93.7 us (99%)
    pallas_call x1, Pallas kernels, shards(): pl.pallas_call(functools.partial(block_kernel, n, m), out_shape=tuple((ja...  90.8 us
    pallas_call x1, Pallas kernels, shards(): pl.pallas_call(place_kernel, out_shape=tuple((jax.ShapeDtypeStruct(s, d)...  2.89 us

profile of v2, /device:TPU:0, one launch (start us, length us, event | category | flops | bytes accessed | tf_op | source)
XLA Modules:
  0.0 94.3 jit_solution(18011405326232504035)
XLA Ops:
  0.6 90.8 %shard_map.198 = (bf16[1,2048,512]{2,1,0:T(8,128)(2,1)S(1)}, bf16[1,2048,512]{2,1,0:T(8,128)(2,1)S(1)}, bf16[1,512,2048]{2,1,0:T(8,128)(2,1)S(1)}, f32[256,256]{...) custom-call(bf16[128,2048]{1,0:T(8,128)(2,1)} %nrm.1, ...), custom_call_target="tpu_custom_call" | custom-call | tf_op jit(solution)/shard_map/pallas_call | solution.py:683
  91.4 2.9 %shard_map.199 = (bf16[1,2048,512]{2,1,0:T(8,128)(2,1)}, bf16[1,2048,512]{2,1,0:T(8,128)(2,1)}, bf16[1,512,2048]{2,1,0:T(8,128)(2,1)}, f32[256,256]{1,0:T(8,128)...) custom-call(bf16[1,2048,512]{2,1,0:T(8,128)(2,1)S(1)} %get-tuple-element.14.refs_0_, ...), custom_call_target="tpu_custom_call" | custom-call | tf_op jit(solution)/shard_map/pallas_call | solution.py:693

commit v3 on v2

--- a/solution.py
+++ b/solution.py
@@ -85,9 +85,9 @@
     ggate, gup, gdown, gow, g_rec, g_dec, g_in,
     xo, co, rtv, pbv, irv, gnv, riv, rgv, igv, dcv, exv, omv, gwv, uwv, dwv,
     info, keep, scin, admit, retain, cum, loc, prev, hid, carry, enters,
-    xg, yg, act, dg, du, pr, stage, red, back, out, hid_all, mix_t, got,
-    ld, zs, zr, xs, f1r, f2r, ds, dr, ns, nr, cs, cr, hs, hr, rs, rr, bs, br,
-    gs, gr, ms, mr, es, er,
+    xg, yg, act, dg, du, pr, st1, mid, st2, red, back, out, hid_all, mix_t, got,
+    ld, zs, zr, xs, f1r, f2r, ds, dr, ns, nr, cs, cr, hs, hr, q1, r1, q2, r2, bs, br,
+    gs, gr, ms, mr, us, ur, es, er,
 ):
     me, j = lax.axis_index("sp"), lax.axis_index("tp")
     tok, feats = nrm.shape
@@ -298,29 +298,60 @@
             part = lax.dot_general(dg[land, :], gwv[f, :], COLDIMS, preferred_element_type=F32)
             part += lax.dot_general(du[land, :], uwv[f, :], COLDIMS, preferred_element_type=F32)
             pr[land, f] = part.astype(BF16)
-        for p in range(1, m):
-            far = lax.rem(j + p, m)
-            send(
-                pr.at[land, cols(far)], stage.at[p - 1, land], rs.at[s], rr.at[s], {"tp": far}
-            ).start()
-
-    def shipped(s):
-        return send(red.at[rows(s)], back.at[rows(me)], bs, br.at[me], {"sp": s})
+
+    parts = 2 if q % 256 == 0 else 1
+    piece = lambda v: pl.ds(v * (q // parts), q // parts)
+
+    def shipped(s, v):
+        return send(
+            red.at[rows(s), piece(v)], back.at[rows(me), piece(v)], bs, br.at[v, me], {"sp": s}
+        )
+
+    def half_sums(s):
+        for h in range(2):
+            for p in range(1, size(h)):
+                for c in range(size(1 - h)):
+                    send(
+                        pr.at[rows(2 * s + h), cols(near(h, p, c))],
+                        st1.at[h, p - 1, c, rows(s)],
+                        q1.at[h],
+                        r1.at[h, s],
+                        {"tp": near(h, p, 0)},
+                    ).start()
+
+    def middle(s):
+        for h in range(2):
+            if size(h) > 1:
+                part = st1.at[h, pl.ds(0, size(h) - 1), pl.ds(0, size(1 - h)), rows(s)]
+                send(part, part, q1.at[h], r1.at[h, s], {"tp": near(h, 1, 0)}).wait_recv()
+            for c in range(size(1 - h)):
+                total = pr[rows(2 * s + h), cols(near(h, 0, c))].astype(F32)
+                for p in range(1, size(h)):
+                    total = total + st1[h, p - 1, c, rows(s)].astype(F32)
+                mid[h, c, rows(s)] = total.astype(BF16)
+            for c in range(1, size(1 - h)):
+                send(
+                    mid.at[h, c, rows(s)],
+                    st2.at[h, c - 1, rows(s)],
+                    q2.at[h],
+                    r2.at[h, s],
+                    {"tp": near(h, 0, c)},
+                ).start()
 
     def reduce(s):
-        land = rows2(s)
-        block = stage.at[:, land]
-        arrived = send(block, block, rs.at[s], rr.at[s], {"tp": lax.rem(j + 1, m)})
-        arrived.wait_recv()
-        arrived.wait_send()
-        total = pr[land, cols(j)].astype(F32)
-        for p in range(1, m):
-            total = total + stage[p - 1, land].astype(F32)
-        red[land] = total.astype(BF16)
-        for c in range(2):
-            @pl.when(2 * s + c != me)
-            def _():
-                shipped(2 * s + c).start()
+        for h in range(2):
+            if size(1 - h) > 1:
+                part = st2.at[h, pl.ds(0, size(1 - h) - 1), rows(s)]
+                send(part, part, q2.at[h], r2.at[h, s], {"tp": near(h, 0, 1)}).wait_recv()
+            total = mid[h, 0, rows(s)].astype(F32)
+            for c in range(1, size(1 - h)):
+                total = total + st2[h, c - 1, rows(s)].astype(F32)
+            red[rows(2 * s + h)] = total.astype(BF16)
+        for v in range(parts):
+            for h in range(2):
+                @pl.when(2 * s + h != me)
+                def _():
+                    shipped(2 * s + h, v).start()
 
     spot = lax.broadcasted_iota(jnp.int32, (tok, chan), 0)
 
@@ -339,56 +370,107 @@
         prev[...] = jnp.where(spot >= 1, pltpu.roll(states, 1, 0), state)
         hid_all[me] = hid[...]
 
-        def shared(k):
-            to = lax.rem(me + k, n)
-            return send(hid, hid_all.at[me], hs, hr.at[k], {"sp": to})
-
-        def share_hidden(k, _):
-            shared(k).start()
-            return 0
-
-        lax.fori_loop(1, n, share_hidden, 0)
-
-    def step(k, _):
-        @pl.when(jnp.logical_and(k >= 1, k < zn))
-        def _():
-            s = source(k)
+    def share_hidden(k, _):
+        to = lax.rem(me + k, n)
+        send(hid, hid_all.at[me], hs, hr.at[k], {"sp": to}).start()
+        return 0
+
+
+    def passing(s):
+        return jnp.where(s < z, jnp.where(z + 1 < zn, 1, 0), jnp.where(z > 0, 1, 0))
+
+    def take_line(s, i, o):
+        line(i, o, s, True).wait_recv()
+
+        @pl.when(jnp.logical_and(s < z, z + 1 < zn))
+        def _():
+            line(i, o, s, True).start()
+
+        @pl.when(jnp.logical_and(s > z, z > 0))
+        def _():
+            line(i, o, s, False).start()
+
+    compute(z)
+
+    def gather(k, _):
+        s = source(k)
+        passes = passing(s)
+        late = jnp.logical_and(k >= 3, passes == 1)
+
+        @pl.when(jnp.logical_and(k >= 3, passes == 0))
+        def _():
+            relayed(source(k - 2))
+
+        for i, o in arrays:
+            take_line(s, i, o)
+
+            @pl.when(jnp.logical_not(late))
+            def _():
+                onward(s, i, o)
+
+        @pl.when(late)
+        def _():
+            relayed(source(k - 2))
+
+            @pl.when(k == zn - 1)
+            def _():
+                relayed(source(k - 1))
+
             for i, o in arrays:
-                line(i, o, s, True).wait_recv()
-
-                @pl.when(jnp.logical_and(s < z, z + 1 < zn))
-                def _():
-                    line(i, o, s, True).start()
-
-                @pl.when(jnp.logical_and(s > z, z > 0))
-                def _():
-                    line(i, o, s, False).start()
-
                 onward(s, i, o)
 
+        return 0
+
+    lax.fori_loop(1, zn, gather, 0)
+    hidden()
+
+    @pl.when(passing(source(zn - 1)) == 0)
+    def _():
+        relayed(source(zn - 2))
+
+    def middles(g, _):
+        middle(source(g))
+        return 0
+
+    def reduces(g, _):
+        reduce(source(g))
+        return 0
+
+    def experts(k, _):
+        @pl.when(k > 1)
+        def _():
+            whole(source(k - 1))
+
         @pl.when(k == zn - 1)
         def _():
-            hidden()
-
-        @pl.when(jnp.logical_and(k >= 2, k < zn + 1))
-        def _():
-            relayed(source(k - 1))
-
-        @pl.when(k >= 3)
-        def _():
-            whole(source(k - 2))
-
-        @pl.when(jnp.logical_or(k == 0, k >= 3))
-        def _():
-            compute(source(jnp.where(k == 0, 0, k - 2)))
-
-        @pl.when(k >= 3)
-        def _():
-            reduce(source(k - 3))
-
-        return 0
-
-    lax.fori_loop(0, zn + 2, step, 0)
+            relayed(source(k))
+
+            def early(g, _):
+                half_sums(source(g))
+                return 0
+
+            lax.fori_loop(0, zn - 2, early, 0)
+
+        @pl.when(k == zn)
+        def _():
+            lax.fori_loop(1, n, share_hidden, 0)
+
+        @pl.when(k > 1)
+        def _():
+            compute(source(k - 1))
+
+        @pl.when(k == zn)
+        def _():
+            lax.fori_loop(0, zn - 2, middles, 0)
+
+        @pl.when(k >= zn - 1)
+        def _():
+            half_sums(source(k - 1))
+
+        return 0
+
+    lax.fori_loop(1, zn + 1, experts, 0)
+    middle(source(zn - 2))
 
     def wide_grads(t, _):
         f = pl.ds(pl.multiple_of(t * 256, 256), 256)
@@ -401,13 +483,16 @@
         ).astype(BF16)
         return 0
 
-    lax.fori_loop(0, feats // 256, wide_grads, 0)
+    lax.fori_loop(0, zn - 2, reduces, 0)
     for t in range(ff // min(ff, 128)):
         f = pl.ds(t * min(ff, 128), min(ff, 128))
         gdown[0, f, :] = lax.dot_general(
             act[:, f], yg[...], ROWDIMS, preferred_element_type=F32
         ).astype(BF16)
-
+    lax.fori_loop(0, feats // 512, wide_grads, 0)
+    reduce(source(zn - 2))
+    middle(source(zn - 1))
+    lax.fori_loop(feats // 512, feats // 256, wide_grads, 0)
     reduce(source(zn - 1))
     back[rows(me)] = red[rows(me)]
 
@@ -419,23 +504,31 @@
     depth = lax.broadcasted_iota(jnp.int32, (n, cap, tok), 1).astype(F32)
     pick = jnp.where(depth == ranking[:, None, :], 1.0, 0.0).reshape(slots, tok).astype(BF16)
 
-    def collect(k, _):
-        s = lax.rem(me - k + n, n)
-        block = back.at[rows(s)]
-        send(block, block, bs, br.at[s], {"sp": s}).wait_recv()
-        return 0
-
-    lax.fori_loop(1, n, collect, 0)
-    total = lax.dot_general(pick, back[...], ROWDIMS, preferred_element_type=F32)
-    out[:, cols(j)] = total.astype(BF16)
+    for v in range(parts):
+        def collect(k, _):
+            s = lax.rem(me - k + n, n)
+            block = back.at[rows(s), piece(v)]
+            send(block, block, bs, br.at[v, s], {"sp": s}).wait_recv()
+            return 0
+
+        lax.fori_loop(1, n, collect, 0)
+        total = lax.dot_general(pick, back[:, piece(v)], ROWDIMS, preferred_element_type=F32)
+        spread = q // parts
+        fields = lambda t: pl.ds(pl.multiple_of(t * q + v * spread, spread), spread)
+        out[:, fields(j)] = total.astype(BF16)
+        mine = out.at[:, fields(j)]
+        for p in range(1, m):
+            send(mine, mine, gs.at[p], gr.at[v, p], {"tp": lax.rem(j + p, m)}).start()
+    for v in range(parts):
+        spread = q // parts
+        fields = lambda t: pl.ds(pl.multiple_of(t * q + v * spread, spread), spread)
+        for p in range(1, m):
+            far = lax.rem(j - p + m, m)
+            theirs = out.at[:, fields(far)]
+            send(theirs, theirs, gs.at[p], gr.at[v, p], {"tp": far}).wait_recv()
     mine = out.at[:, cols(j)]
     for p in range(1, m):
-        send(mine, mine, gs.at[p], gr.at[p], {"tp": lax.rem(j + p, m)}).start()
-    for p in range(1, m):
-        far = lax.rem(j - p + m, m)
-        theirs = out.at[:, cols(far)]
-        send(mine, mine, gs.at[p], gr.at[p], {"tp": far}).wait_send()
-        send(theirs, theirs, gs.at[p], gr.at[p], {"tp": far}).wait_recv()
+        send(mine, mine, gs.at[p], gr.at[0, p], {"tp": lax.rem(j + p, m)}).wait_send()
 
     slab = feats // n
     slabs = lambda s: pl.ds(pl.multiple_of(s * slab, slab), slab)
@@ -447,13 +540,44 @@
     mixed = co[toks(me)].astype(F32) + root * (gained - nhat * stat)
     mix_t[...] = mixed.T.astype(BF16)
 
-    def blocks(k):
-        to = lax.rem(me + k, n)
-        return send(mix_t.at[slabs(to)], got.at[me], ms, mr.at[k], {"sp": to})
-
-    def start_blocks(k, _):
-        blocks(k).start()
-        return 0
+    def share_of(i):
+        part = slab // size(i)
+        return pl.ds(pl.multiple_of((lower if i == 0 else upper) * part, part), part)
+
+    def start_blocks(i):
+        part = slab // size(i)
+        own = lower if i == 0 else upper
+
+        def start(k, _):
+            to = lax.rem(me + k, n)
+            piece = pl.ds(pl.multiple_of(to * slab + own * part, part), part)
+            send(
+                mix_t.at[piece], got.at[me, share_of(i)], ms, mr.at[me], {"sp": to}
+            ).start()
+            return 0
+
+        lax.fori_loop(1, n, start, 0)
+
+    def pass_block(i, s):
+        block = got.at[s, share_of(i)]
+        send(block, block, ms, mr.at[s], {"sp": s}).wait_recv()
+        for p in range(1, size(i)):
+            send(block, block, us.at[i], ur.at[s], {"tp": near(i, p, 0)}).start()
+
+    def end_block(i, s):
+        if size(i) > 1:
+            block = got.at[s, pl.ds(0, slab // size(i) * (size(i) - 1))]
+            send(block, block, us.at[i], ur.at[s], {"tp": near(i, 1, 0)}).wait_recv()
+        gow[...] += jnp.dot(got[s], hid_all[s], preferred_element_type=F32)
+
+    def on_side(work, s):
+        @pl.when(lax.rem(s, 2) == 0)
+        def _():
+            work(0, s)
+
+        @pl.when(lax.rem(s, 2) == 1)
+        def _():
+            work(1, s)
 
     d_state = jnp.dot(mixed.astype(BF16), omv[...], preferred_element_type=F32)
     here = keep[...]
@@ -472,13 +596,33 @@
         return 0
 
     lax.fori_loop(1, n, start_enter, 0)
-    lax.fori_loop(1, n, start_blocks, 0)
+    @pl.when(par == 0)
+    def _():
+        start_blocks(0)
+
+    @pl.when(par == 1)
+    def _():
+        start_blocks(1)
+
     gow[...] = jnp.dot(mix_t[slabs(me)], hid_all[me], preferred_element_type=F32)
 
     def take_hidden(k, _):
         s = lax.rem(me - k + n, n)
         send(hid, hid_all.at[s], hs, hr.at[k], {"sp": s}).wait_recv()
         return 0
+
+    def nearby(k):
+        return 2 * source(lax.div(k, 2)) + lax.rem(k + par, 2)
+
+    def pass_blocks(k, _):
+        on_side(pass_block, nearby(k))
+        return 0
+
+    def end_blocks(k, _):
+        on_side(end_block, nearby(k))
+        return 0
+
+    lax.fori_loop(1, n, pass_blocks, 0)
 
     def take_enter(k, _):
         s = lax.rem(me - k + n, n)
@@ -499,13 +643,7 @@
 
     lax.fori_loop(1, n, take_hidden, 0)
 
-    def add(k, _):
-        s = lax.rem(me - k + n, n)
-        send(got.at[s], got.at[s], ms, mr.at[k], {"sp": s}).wait_recv()
-        gow[...] += jnp.dot(got[s], hid_all[s], preferred_element_type=F32)
-        return 0
-
-    lax.fori_loop(1, n, add, 0)
+    lax.fori_loop(1, n, end_blocks, 0)
 
     def flush(s, _):
         for i, o in arrays:
@@ -525,15 +663,49 @@
         send(part, part, xs.at[i], f1r.at[i, 0], {"tp": lax.rem(j + 1, m)}).wait_send()
         part = o.at[pl.ds(0, zn * tok)]
         send(part, part, ds.at[i], dr.at[i, 0], {"sp": partner}).wait_send()
+    for h in range(2):
+        if size(h) > 1:
+            part = st1.at[h, pl.ds(0, size(h) - 1), pl.ds(0, size(1 - h))]
+            send(part, part, q1.at[h], r1.at[h, 0], {"tp": near(h, 1, 0)}).wait_send()
+        if size(1 - h) > 1:
+            part = st2.at[h, pl.ds(0, size(1 - h) - 1)]
+            send(part, part, q2.at[h], r2.at[h, 0], {"tp": near(h, 0, 1)}).wait_send()
     to = {"sp": partner}
     others = pl.ds(0, n - 1)
     send(info.at[others], info.at[others], ns, nr.at[0], to).wait_send()
     send(carry.at[others], carry.at[others], cs, cr.at[0], to).wait_send()
     send(enters.at[others], enters.at[others], es, er.at[0], to).wait_send()
     send(hid_all.at[others], hid_all.at[others], hs, hr.at[0], to).wait_send()
-    send(got.at[others], got.at[others], ms, mr.at[0], to).wait_send()
+
+    def flush_blocks(i):
+        part = slab // size(i)
+        block = got.at[others, pl.ds(0, part)]
+        send(block, block, ms, mr.at[0], to).wait_send()
+
+    @pl.when(par == 0)
+    def _():
+        flush_blocks(0)
+
+    @pl.when(par == 1)
+    def _():
+        flush_blocks(1)
+
+    for i in range(2):
+        if size(i) > 1:
+            part = slab // size(i) * (size(i) - 1)
+            half_of = got.at[pl.ds(0, zn), pl.ds(0, part)]
+            less = got.at[pl.ds(0, zn - 1), pl.ds(0, part)]
+
+            @pl.when(par == i)
+            def _():
+                send(less, less, us.at[i], ur.at[0], {"tp": near(i, 1, 0)}).wait_send()
+
+            @pl.when(par != i)
+            def _():
+                send(half_of, half_of, us.at[i], ur.at[0], {"tp": near(i, 1, 0)}).wait_send()
+
     part = red.at[pl.ds(0, (n - 1) * cap)]
-    send(part, part, bs, br.at[0], to).wait_send()
+    send(part, part, bs, br.at[0, 0], to).wait_send()
 
 
 def place_kernel(*refs):
@@ -585,6 +757,7 @@
     ff = gate_weight.shape[2]
     chan = recurrence_input.shape[1]
     zn = n // 2
+    wide = max(sides(m))
     dma = pltpu.SemaphoreType.DMA
     vmem = lambda *s: pltpu.VMEM(s, F32)
     half = lambda *s: pltpu.VMEM(s, BF16)
@@ -630,7 +803,9 @@
         half(slots, ff),
         half(slots, ff),
         half(slots, feats),
-        half(m - 1, slots, q),
+        half(2, max(wide - 1, 1), wide, zn * cap, q),
+        half(2, wide, zn * cap, q),
+        half(2, max(wide - 1, 1), zn * cap, q),
         half(slots, q),
         half(slots, q),
         half(tok, feats),
@@ -651,13 +826,17 @@
         dma((n,)),
         dma,
         dma((n,)),
-        dma((zn,)),
-        dma((zn,)),
+        dma((2,)),
+        dma((2, zn)),
+        dma((2,)),
+        dma((2, zn)),
+        dma,
+        dma((2, n)),
+        dma((m,)),
+        dma((2, m)),
         dma,
         dma((n,)),
-        dma((m,)),
-        dma((m,)),
-        dma,
+        dma((2,)),
         dma((n,)),
         dma,
         dma((n,)),

time: 94.5 us -> 91 us (0.963)
  Pallas kernels: 93.7 us -> 90.2 us
    pallas_call x1, Pallas kernels: 90.8 us -> 87.3 us  [shards(): pl.pallas_call(functools.partial(block_kernel, n, m), out_shape=tuple((ja...]
where the time goes in v3:
time: 91 us; the launch traced here: 90.8 us
  Pallas kernels  90.2 us (99%)
    pallas_call x1, Pallas kernels, shards(): pl.pallas_call(functools.partial(block_kernel, n, m), out_shape=tuple((ja...  87.3 us
    pallas_call x1, Pallas kernels, shards(): pl.pallas_call(place_kernel, out_shape=tuple((jax.ShapeDtypeStruct(s, d)...  2.89 us

profile of v3, /device:TPU:0, one launch (start us, length us, event | category | flops | bytes accessed | tf_op | source)
XLA Modules:
  0.0 90.8 jit_solution(5175972948033305333)
XLA Ops:
  0.6 87.3 %shard_map.198 = (bf16[1,2048,512]{2,1,0:T(8,128)(2,1)S(1)}, bf16[1,2048,512]{2,1,0:T(8,128)(2,1)S(1)}, bf16[1,512,2048]{2,1,0:T(8,128)(2,1)S(1)}, f32[256,256]{...) custom-call(bf16[128,2048]{1,0:T(8,128)(2,1)} %nrm.1, ...), custom_call_target="tpu_custom_call" | custom-call | tf_op jit(solution)/shard_map/pallas_call | solution.py:862
  88.0 2.9 %shard_map.199 = (bf16[1,2048,512]{2,1,0:T(8,128)(2,1)}, bf16[1,2048,512]{2,1,0:T(8,128)(2,1)}, bf16[1,512,2048]{2,1,0:T(8,128)(2,1)}, f32[256,256]{1,0:T(8,128)...) custom-call(bf16[1,2048,512]{2,1,0:T(8,128)(2,1)S(1)} %get-tuple-element.14.refs_0_, ...), custom_call_target="tpu_custom_call" | custom-call | tf_op jit(solution)/shard_map/pallas_call | solution.py:872

commit v4 on v3

--- a/solution.py
+++ b/solution.py
@@ -85,9 +85,9 @@
     ggate, gup, gdown, gow, g_rec, g_dec, g_in,
     xo, co, rtv, pbv, irv, gnv, riv, rgv, igv, dcv, exv, omv, gwv, uwv, dwv,
     info, keep, scin, admit, retain, cum, loc, prev, hid, carry, enters,
-    xg, yg, act, dg, du, pr, st1, mid, st2, red, back, out, hid_all, mix_t, got,
+    xg, yg, act, dg, du, pr, st1, mid, st2, red, back, out, hid_all, mix_t, got, stats, nh_t,
     ld, zs, zr, xs, f1r, f2r, ds, dr, ns, nr, cs, cr, hs, hr, q1, r1, q2, r2, bs, br,
-    gs, gr, ms, mr, us, ur, es, er,
+    gs, gr, ms, mr, us, ur, es, er, ws, wr,
 ):
     me, j = lax.axis_index("sp"), lax.axis_index("tp")
     tok, feats = nrm.shape
@@ -390,7 +390,7 @@
         def _():
             line(i, o, s, False).start()
 
-    compute(z)
+    turn = jnp.where(jnp.logical_or(z == 0, z == zn - 1), 1, 2)
 
     def gather(k, _):
         s = source(k)
@@ -418,6 +418,10 @@
 
             for i, o in arrays:
                 onward(s, i, o)
+
+        @pl.when(k == turn)
+        def _():
+            compute(z)
 
         return 0
 
@@ -489,12 +493,26 @@
         gdown[0, f, :] = lax.dot_general(
             act[:, f], yg[...], ROWDIMS, preferred_element_type=F32
         ).astype(BF16)
+    middle(source(zn - 1))
     lax.fori_loop(0, feats // 512, wide_grads, 0)
     reduce(source(zn - 2))
-    middle(source(zn - 1))
-    lax.fori_loop(feats // 512, feats // 256, wide_grads, 0)
     reduce(source(zn - 1))
     back[rows(me)] = red[rows(me)]
+    lax.fori_loop(feats // 512, feats // 256, wide_grads, 0)
+
+    slab = feats // n
+    slabs = lambda s: pl.ds(pl.multiple_of(s * slab, slab), slab)
+    window = nh_t.shape[1]
+    base = lax.div(me * slab, window)
+    band = pl.ds(pl.multiple_of(base * window, window), window)
+    inside = pl.ds(pl.multiple_of(me * slab - base * window, slab), slab)
+
+    def turned(s, _):
+        nh_t[s] = (xo[toks(s), band].astype(F32) / gnv[:, band]).T.astype(BF16)
+        return 0
+
+    lax.fori_loop(0, n, turned, 0)
+    root = jnp.broadcast_to(irv[...], (8, tok)).T[:, 0:1]
 
     own = info[me]
     experts = lax.broadcasted_iota(jnp.int32, (n, tok), 0).astype(F32)
@@ -519,6 +537,27 @@
         mine = out.at[:, fields(j)]
         for p in range(1, m):
             send(mine, mine, gs.at[p], gr.at[v, p], {"tp": lax.rem(j + p, m)}).start()
+    def share_of(i):
+        part = slab // size(i)
+        return pl.ds(pl.multiple_of((lower if i == 0 else upper) * part, part), part)
+
+    def start_blocks(i, v):
+        part = slab // size(i)
+        own = lower if i == 0 else upper
+
+        def start(k, _):
+            to = lax.rem(me + k, n)
+            last = lax.div(lax.rem(to * slab, q) + slab - 1, q // parts)
+            block = pl.ds(pl.multiple_of(to * slab + own * part, part), part)
+
+            @pl.when(last == v)
+            def _():
+                send(mix_t.at[block], got.at[me, share_of(i)], ms, mr.at[me], {"sp": to}).start()
+
+            return 0
+
+        lax.fori_loop(1, n, start, 0)
+
     for v in range(parts):
         spread = q // parts
         fields = lambda t: pl.ds(pl.multiple_of(t * q + v * spread, spread), spread)
@@ -526,37 +565,36 @@
             far = lax.rem(j - p + m, m)
             theirs = out.at[:, fields(far)]
             send(theirs, theirs, gs.at[p], gr.at[v, p], {"tp": far}).wait_recv()
+        for t in range(m):
+            f = pl.ds(t * q + v * spread, spread)
+            most = co[toks(me), f].astype(F32) + root * (gnv[:, f] * out[:, f].astype(F32))
+            mix_t[f, :] = most.T.astype(BF16)
+
+        @pl.when(par == 0)
+        def _():
+            start_blocks(0, v)
+
+        @pl.when(par == 1)
+        def _():
+            start_blocks(1, v)
+
     mine = out.at[:, cols(j)]
     for p in range(1, m):
         send(mine, mine, gs.at[p], gr.at[0, p], {"tp": lax.rem(j + p, m)}).wait_send()
 
-    slab = feats // n
-    slabs = lambda s: pl.ds(pl.multiple_of(s * slab, slab), slab)
     scale = gnv[...]
     nhat = xo[toks(me)].astype(F32) / scale
     gained = scale * out[...].astype(F32)
     stat = jnp.mean(gained * nhat, axis=1, keepdims=True)
-    root = jnp.broadcast_to(irv[...], (8, tok)).T[:, 0:1]
     mixed = co[toks(me)].astype(F32) + root * (gained - nhat * stat)
-    mix_t[...] = mixed.T.astype(BF16)
-
-    def share_of(i):
-        part = slab // size(i)
-        return pl.ds(pl.multiple_of((lower if i == 0 else upper) * part, part), part)
-
-    def start_blocks(i):
-        part = slab // size(i)
-        own = lower if i == 0 else upper
-
-        def start(k, _):
-            to = lax.rem(me + k, n)
-            piece = pl.ds(pl.multiple_of(to * slab + own * part, part), part)
-            send(
-                mix_t.at[piece], got.at[me, share_of(i)], ms, mr.at[me], {"sp": to}
-            ).start()
-            return 0
-
-        lax.fori_loop(1, n, start, 0)
+    stats[me] = jnp.broadcast_to(root * stat, (tok, 128)).T[0:8]
+
+    def start_stats(k, _):
+        to = lax.rem(me + k, n)
+        send(stats.at[me], stats.at[me], ws, wr.at[me], {"sp": to}).start()
+        return 0
+
+    lax.fori_loop(1, n, start_stats, 0)
 
     def pass_block(i, s):
         block = got.at[s, share_of(i)]
@@ -568,7 +606,9 @@
         if size(i) > 1:
             block = got.at[s, pl.ds(0, slab // size(i) * (size(i) - 1))]
             send(block, block, us.at[i], ur.at[s], {"tp": near(i, 1, 0)}).wait_recv()
-        gow[...] += jnp.dot(got[s], hid_all[s], preferred_element_type=F32)
+        send(stats.at[s], stats.at[s], ws, wr.at[s], {"sp": s}).wait_recv()
+        left = got[s].astype(F32) - nh_t[s, inside, :].astype(F32) * stats[s][0:1]
+        gow[...] += jnp.dot(left.astype(BF16), hid_all[s], preferred_element_type=F32)
 
     def on_side(work, s):
         @pl.when(lax.rem(s, 2) == 0)
@@ -596,15 +636,8 @@
         return 0
 
     lax.fori_loop(1, n, start_enter, 0)
-    @pl.when(par == 0)
-    def _():
-        start_blocks(0)
-
-    @pl.when(par == 1)
-    def _():
-        start_blocks(1)
-
-    gow[...] = jnp.dot(mix_t[slabs(me)], hid_all[me], preferred_element_type=F32)
+    left = mix_t[slabs(me)].astype(F32) - nh_t[me, inside, :].astype(F32) * stats[me][0:1]
+    gow[...] = jnp.dot(left.astype(BF16), hid_all[me], preferred_element_type=F32)
 
     def take_hidden(k, _):
         s = lax.rem(me - k + n, n)
@@ -675,6 +708,7 @@
     send(info.at[others], info.at[others], ns, nr.at[0], to).wait_send()
     send(carry.at[others], carry.at[others], cs, cr.at[0], to).wait_send()
     send(enters.at[others], enters.at[others], es, er.at[0], to).wait_send()
+    send(stats.at[others], stats.at[others], ws, wr.at[0], to).wait_send()
     send(hid_all.at[others], hid_all.at[others], hs, hr.at[0], to).wait_send()
 
     def flush_blocks(i):
@@ -812,6 +846,8 @@
         half(n, tok, chan),
         half(feats, tok),
         half(n, feats // n, tok),
+        vmem(n, 8, tok),
+        half(n, max(feats // n, 128), tok),
         dma((15,)),
         dma((2, 2, zn)),
         dma((2, zn)),
@@ -837,6 +873,8 @@
         dma,
         dma((n,)),
         dma((2,)),
+        dma((n,)),
+        dma,
         dma((n,)),
         dma,
         dma((n,)),

time: 91 us -> 89.3 us (0.981)
  Pallas kernels: 90.2 us -> 88.5 us
    pallas_call x1, Pallas kernels: 87.3 us -> 85.6 us  [shards(): pl.pallas_call(functools.partial(block_kernel, n, m), out_shape=tuple((ja...]
where the time goes in v4:
time: 89.3 us; the launch traced here: 89.1 us
  Pallas kernels  88.5 us (99%)
    pallas_call x1, Pallas kernels, shards(): pl.pallas_call(functools.partial(block_kernel, n, m), out_shape=tuple((ja...  85.6 us
    pallas_call x1, Pallas kernels, shards(): pl.pallas_call(place_kernel, out_shape=tuple((jax.ShapeDtypeStruct(s, d)...  2.89 us

profile of v4, /device:TPU:0, one launch (start us, length us, event | category | flops | bytes accessed | tf_op | source)
XLA Modules:
  0.0 89.1 jit_solution(10502677265334051875)
XLA Ops:
  0.6 85.6 %shard_map.198 = (bf16[1,2048,512]{2,1,0:T(8,128)(2,1)S(1)}, bf16[1,2048,512]{2,1,0:T(8,128)(2,1)S(1)}, bf16[1,512,2048]{2,1,0:T(8,128)(2,1)S(1)}, f32[256,256]{...) custom-call(bf16[128,2048]{1,0:T(8,128)(2,1)} %nrm.1, ...), custom_call_target="tpu_custom_call" | custom-call | tf_op jit(solution)/shard_map/pallas_call | solution.py:900
  86.2 2.9 %shard_map.199 = (bf16[1,2048,512]{2,1,0:T(8,128)(2,1)}, bf16[1,2048,512]{2,1,0:T(8,128)(2,1)}, bf16[1,512,2048]{2,1,0:T(8,128)(2,1)}, f32[256,256]{1,0:T(8,128)...) custom-call(bf16[1,2048,512]{2,1,0:T(8,128)(2,1)S(1)} %get-tuple-element.14.refs_0_, ...), custom_call_target="tpu_custom_call" | custom-call | tf_op jit(solution)/shard_map/pallas_call | solution.py:910

commit v5 on v4

--- a/solution.py
+++ b/solution.py
@@ -85,7 +85,7 @@
     ggate, gup, gdown, gow, g_rec, g_dec, g_in,
     xo, co, rtv, pbv, irv, gnv, riv, rgv, igv, dcv, exv, omv, gwv, uwv, dwv,
     info, keep, scin, admit, retain, cum, loc, prev, hid, carry, enters,
-    xg, yg, act, dg, du, pr, st1, mid, st2, red, back, out, hid_all, mix_t, got, stats, nh_t,
+    xg, yg, gates, ups, act, dg, du, pr, st1, mid, st2, red, back, out, hid_all, mix_t, got, stats, nh_t,
     ld, zs, zr, xs, f1r, f2r, ds, dr, ns, nr, cs, cr, hs, hr, q1, r1, q2, r2, bs, br,
     gs, gr, ms, mr, us, ur, es, er, ws, wr,
 ):
@@ -231,8 +231,13 @@
     for at in range(9, 15):
         loads[at].wait()
 
+    def beside(s, i, o, t):
+        block = o.at[toks(2 * s + par), cols(t)]
+        send(block, block, ds.at[i], dr.at[i, s], {"sp": partner}).start()
+
     def onward(s, i, o):
         block = o.at[toks(2 * s + par), cols(j)]
+        beside(s, i, o, j)
         for p in range(1, size(i)):
             send(block, block, xs.at[i], f1r.at[i, s], {"tp": near(i, p, 0)}).start()
         for p in range(1, size(1 - i)):
@@ -248,6 +253,7 @@
                 send(part, part, xs.at[i], f1r.at[i, s], {"tp": near(i, 1, 0)}).wait_recv()
             for c in range(1, size(i)):
                 block = o.at[toks(2 * s + par), cols(near(i, size(i) - c, 0))]
+                beside(s, i, o, near(i, size(i) - c, 0))
                 for p in range(1, size(1 - i)):
                     send(block, block, xs.at[i], f2r.at[i, s], {"tp": near(i, 0, p)}).start()
 
@@ -256,16 +262,20 @@
             if size(1 - i) > 1:
                 part = several(o, s, m - size(i))
                 send(part, part, xs.at[i], f2r.at[i, s], {"tp": near(i, 0, 1)}).wait_recv()
-            across(i, o, s).start()
+            for c in range(1, size(1 - i)):
+                for p in range(size(i)):
+                    beside(s, i, o, near(i, p, c))
 
     span = min(feats, 512)
     unit = min(ff, 256)
 
     def compute(s):
         other = 2 * s + 1 - par
-        for i, o in arrays:
+
+        def arrive(i, o):
             block = o.at[toks(other)]
             send(block, block, ds.at[i], dr.at[i, s], {"sp": partner}).wait_recv()
+
         (low_at, low_weight), (high_at, high_weight) = place(2 * s), place(2 * s + 1)
         high_at = jnp.where(high_at >= 0.0, high_at + float(cap), -1.0)
         at = jnp.concatenate([low_at, high_at], axis=1)
@@ -277,16 +287,23 @@
         one = one.astype(BF16)
         pair = pl.ds(pl.multiple_of(s * 2 * tok, 2 * tok), 2 * tok)
         land = rows2(s)
+        arrive(0, xo)
         for t in range(feats // span):
             f = pl.ds(t * span, span)
             xg[land, f] = jnp.dot(one, xo[pair, f], preferred_element_type=F32).astype(BF16)
+        for t in range(ff // unit):
+            f = pl.ds(t * unit, unit)
+            gates[:, f] = jnp.dot(xg[land, :], gwv[:, f], preferred_element_type=F32)
+            ups[:, f] = jnp.dot(xg[land, :], uwv[:, f], preferred_element_type=F32)
+        arrive(1, co)
+        for t in range(feats // span):
+            f = pl.ds(t * span, span)
             yg[land, f] = (share * jnp.dot(one, co[pair, f], preferred_element_type=F32)).astype(
                 BF16
             )
         for t in range(ff // unit):
             f = pl.ds(t * unit, unit)
-            gate = jnp.dot(xg[land, :], gwv[:, f], preferred_element_type=F32)
-            up = jnp.dot(xg[land, :], uwv[:, f], preferred_element_type=F32)
+            gate, up = gates[:, f], ups[:, f]
             d_act = lax.dot_general(yg[land, :], dwv[f, :], COLDIMS, preferred_element_type=F32)
             sigma = jax.nn.sigmoid(gate)
             swish = gate * sigma
@@ -833,6 +850,8 @@
         vmem(n, 8, chan),
         half(slots, feats),
         half(slots, feats),
+        vmem(2 * cap, ff),
+        vmem(2 * cap, ff),
         half(slots, ff),
         half(slots, ff),
         half(slots, ff),

time: 89.3 us -> 89.5 us (level)
  no operation moved by 1% of the time
where the time goes in v5:
time: 89.5 us; the launch traced here: 89.4 us
  Pallas kernels  88.7 us (99%)
    pallas_call x1, Pallas kernels, shards(): pl.pallas_call(functools.partial(block_kernel, n, m), out_shape=tuple((ja...  85.8 us
    pallas_call x1, Pallas kernels, shards(): pl.pallas_call(place_kernel, out_shape=tuple((jax.ShapeDtypeStruct(s, d)...  2.89 us

profile of v5, /device:TPU:0, one launch (start us, length us, event | category | flops | bytes accessed | tf_op | source)
XLA Modules:
  0.0 89.4 jit_solution(1552660318555447705)
XLA Ops:
  0.6 85.8 %shard_map.198 = (bf16[1,2048,512]{2,1,0:T(8,128)(2,1)S(1)}, bf16[1,2048,512]{2,1,0:T(8,128)(2,1)S(1)}, bf16[1,512,2048]{2,1,0:T(8,128)(2,1)S(1)}, f32[256,256]{...) custom-call(bf16[128,2048]{1,0:T(8,128)(2,1)} %nrm.1, ...), custom_call_target="tpu_custom_call" | custom-call | tf_op jit(solution)/shard_map/pallas_call | solution.py:919
  86.5 2.9 %shard_map.199 = (bf16[1,2048,512]{2,1,0:T(8,128)(2,1)}, bf16[1,2048,512]{2,1,0:T(8,128)(2,1)}, bf16[1,512,2048]{2,1,0:T(8,128)(2,1)}, f32[256,256]{1,0:T(8,128)...) custom-call(bf16[1,2048,512]{2,1,0:T(8,128)(2,1)S(1)} %get-tuple-element.14.refs_0_, ...), custom_call_target="tpu_custom_call" | custom-call | tf_op jit(solution)/shard_map/pallas_call | solution.py:929
